TPU v7x, 32 devices: a whole 2x2x4 slice. The times are simulated.
32 devices in a mesh: sp: 8 (over z, y), tp: 4 (over x, core).
Axes of the slice: x: 2, y: 2, z: 4, core: 2. Of those that a mesh axis runs over, the one named last changes fastest.
Arguments:
- resid: bfloat16 [8192, 2048], P(('sp', 'tp')), may hold values from -6 to 6
- queries: bfloat16 [8192, 2048], P('sp', 'tp'), may hold values from -6 to 6
- keys: bfloat16 [8192, 2048], P('sp', 'tp'), may hold values from -6 to 6
- values: bfloat16 [8192, 4096], P('sp', 'tp'), may hold values from -6 to 6
- gates: bfloat16 [8192, 4096], P('sp', 'tp'), may hold values from -6 to 6
- log_decay: float32 [8, 8192], P('tp', 'sp'), may hold values from -1 to 0
- retention_output_weight: bfloat16 [4096, 2048], P('tp'), may hold values from -0.125 to 0.125
- norm_gain: bfloat16 [2048], replicated, may hold values from 0.099609375 to 1.8984375
- up_weight: bfloat16 [2048, 8192], P('sp', 'tp'), may hold values from -0.125 to 0.125
- down_weight: bfloat16 [8192, 2048], P('tp', 'sp'), may hold values from -0.0625 to 0.0625
Outputs:
- layer_out: bfloat16 [8192, 2048], P(('sp', 'tp'))
All inputs are finite; a program needn't handle non-finite values.
Results may differ from a plain program's by a relative error of at most 0.02.
Values may be sent and summed in bfloat16 or wider, within the bound.
No kernel may reach another device: no remote copies, remote signals or barrier semaphores. Data moves between devices by JAX's collectives and lax.ppermute only.
A program may use at most 128 MiB of HBM per device.

v0:
```python
import jax
import jax.numpy as jnp
from jax import lax
from jax.sharding import PartitionSpec as P

DK = 256
DV = 512
BLOCK = 128


tiny_stabilizer = 1e-06


def carried_in(value, axis, combine, identity):
    length, position = (lax.axis_size(axis), lax.axis_index(axis))
    everything = jax.tree.map(
        lambda part, kind: lax.all_gather(part.astype(kind), axis),
        value,
        (jnp.bfloat16, jnp.bfloat16),
    )
    start = jax.tree.map(
        lambda part, zero: jnp.broadcast_to(jnp.asarray(zero, part.dtype), part.shape),
        value,
        identity,
    )

    def turn(k, before):
        reached = k < position
        new = combine(
            before, jax.tree.map(lambda part, own: part[k].astype(own.dtype), everything, value)
        )
        return jax.tree.map(lambda a, b: jnp.where(reached, a, b), new, before)

    return lax.fori_loop(0, length, turn, start)


def rotate(values_in, token_indices):
    half_width = values_in.shape[-1] // 2
    inverse = 10000.0 ** (-jnp.arange(0, 2 * half_width, 2, dtype=jnp.float32) / (2 * half_width))
    angles = token_indices[:, None].astype(jnp.float32) * inverse[None, :]
    cosine = jnp.cos(angles)[:, None, :]
    sine_lookup = jnp.sin(angles)[:, None, :]
    first_half = values_in[..., :half_width]
    second = values_in[..., half_width:]
    return jnp.concatenate(
        [first_half * cosine - second * sine_lookup, first_half * sine_lookup + second * cosine],
        axis=-1,
    )


def normalize(updated, norm_gain):
    widened = updated.astype(jnp.float32)
    scaled = widened * lax.rsqrt(
        jnp.mean(widened * widened, axis=-1, keepdims=True) + tiny_stabilizer
    )
    return (scaled * norm_gain.astype(jnp.float32)).astype(jnp.bfloat16)


def activate(preact):
    positive = jnp.maximum(preact, 0.0)
    return (positive * positive).astype(jnp.bfloat16)


def combine(earlier, later):
    return (earlier[0] * later[0], later[0][:, None, None] * earlier[1] + later[1])


def carry_step(prior, inputs):
    term, decay = inputs
    return (decay[:, None, None] * prior + term, prior)


def retention(queries, keys, values, gates, log_decay):
    row_count = queries.shape[0]
    local_heads = log_decay.shape[0]
    blocks = row_count // BLOCK
    token_indices = lax.axis_index("sp") * row_count + jnp.arange(row_count, dtype=jnp.int32)
    query_rot = rotate(
        queries.reshape(row_count, local_heads, DK).astype(jnp.float32), token_indices
    )
    query_rot = query_rot.astype(jnp.bfloat16).reshape(blocks, BLOCK, local_heads, DK)
    key_rot = rotate(
        keys.reshape(row_count, local_heads, DK).astype(jnp.float32), token_indices
    ) * DK ** (-0.5)
    key_rot = key_rot.astype(jnp.bfloat16).reshape(blocks, BLOCK, local_heads, DK)
    value_blk = values.reshape(blocks, BLOCK, local_heads, DV)
    gate_blk = gates.reshape(blocks, BLOCK, local_heads, DV)
    cumulative = jnp.cumsum(log_decay.reshape(local_heads, blocks, BLOCK), axis=2)
    causal = jnp.arange(BLOCK)[:, None] >= jnp.arange(BLOCK)[None, :]
    spread = cumulative[:, :, :, None] - cumulative[:, :, None, :]
    factor = jnp.where(causal, jnp.exp(jnp.minimum(spread, 0.0)), 0.0)
    scores = jnp.einsum("nihd,njhd->hnij", query_rot, key_rot, preferred_element_type=jnp.float32)
    weights = (scores * factor).astype(jnp.bfloat16)
    within_block = jnp.einsum(
        "hnij,njhv->nihv", weights, value_blk, preferred_element_type=jnp.float32
    )
    tile_count_all = cumulative[:, :, -1]
    to_end = jnp.transpose(jnp.exp(tile_count_all[:, :, None] - cumulative), (1, 2, 0))[..., None]
    key_decayed = (key_rot * to_end).astype(jnp.bfloat16)
    block_terms = jnp.einsum(
        "njhd,njhv->nhdv", key_decayed, value_blk, preferred_element_type=jnp.float32
    )
    local_state, from_local = lax.scan(
        carry_step,
        jnp.zeros((local_heads, DK, DV), jnp.float32),
        (block_terms, jnp.exp(tile_count_all).T),
    )
    device_decay = jnp.exp(jnp.sum(tile_count_all, axis=1))
    identity = (
        jnp.ones((local_heads,), jnp.float32),
        jnp.zeros((local_heads, DK, DV), jnp.float32),
    )
    unused, incoming = carried_in((device_decay, local_state), "sp", combine, identity)
    before = jnp.exp(jnp.cumsum(tile_count_all, axis=1) - tile_count_all).T
    states = (before[:, :, None, None] * incoming[None] + from_local).astype(jnp.bfloat16)
    from_start = jnp.transpose(jnp.exp(cumulative), (1, 2, 0))[..., None]
    query_decayed = (query_rot * from_start).astype(jnp.bfloat16)
    carried_part = jnp.einsum(
        "nihd,nhdv->nihv", query_decayed, states, preferred_element_type=jnp.float32
    )
    retained = within_block + carried_part
    normed = retained * lax.rsqrt(
        jnp.mean(retained * retained, axis=-1, keepdims=True) + tiny_stabilizer
    )
    gated_out = (jax.nn.silu(gate_blk.astype(jnp.float32)) * normed).astype(jnp.bfloat16)
    return gated_out.reshape(row_count, local_heads * DV)


def body(
    resid,
    queries,
    keys,
    values,
    gates,
    log_decay,
    retention_output_weight,
    norm_gain,
    up_weight,
    down_weight,
):
    gated_out = retention(queries, keys, values, gates, log_decay)
    mixed_sum = lax.psum_scatter(
        jnp.dot(gated_out, retention_output_weight, preferred_element_type=jnp.float32).astype(
            jnp.bfloat16
        ),
        "tp",
        scatter_dimension=0,
        tiled=True,
    ).astype(jnp.float32)
    updated = (resid.astype(jnp.float32) + mixed_sum).astype(jnp.bfloat16)
    normed_whole = lax.all_gather(normalize(updated, norm_gain), "tp", axis=0, tiled=True)
    preact = jnp.dot(
        normed_whole,
        lax.all_gather(up_weight, "sp", axis=0, tiled=True),
        preferred_element_type=jnp.float32,
    )
    hidden = activate(preact)
    partial_sums = jnp.dot(
        hidden,
        lax.all_gather(down_weight, "sp", axis=1, tiled=True),
        preferred_element_type=jnp.float32,
    )
    channel_sum = lax.psum_scatter(
        partial_sums.astype(jnp.bfloat16), "tp", scatter_dimension=0, tiled=True
    ).astype(jnp.float32)
    return (updated.astype(jnp.float32) + channel_sum).astype(jnp.bfloat16)


def solution(mesh):
    placed = (
        P(("sp", "tp"), None),
        P("sp", "tp"),
        P("sp", "tp"),
        P("sp", "tp"),
        P("sp", "tp"),
        P("tp", "sp"),
        P("tp", None),
        P(),
        P("sp", "tp"),
        P("tp", "sp"),
    )
    return jax.shard_map(
        body, mesh=mesh, in_specs=placed, out_specs=P(("sp", "tp"), None), check_vma=False
    )
```

profile of v0, /device:TPU:0, one launch (start us, length us, event | category | flops | bytes accessed | tf_op | source)
XLA Modules:
  0.0 582.5 jit_solution(4600715882606489682)
XLA Ops:
  6.6 2.3 copy.63
  10.3 2.3 copy.68
  14.1 1.9 multiply_cosine_fusion
  15.9 2.5 subtract_convert_fusion
  18.5 2.5 copy.69
  21.0 2.6 copy.70
  24.6 3.3 reshape.135
  28.0 6.6 %fusion.12 = f32[8,2,256,512]{3,2,1,0:T(8,128)} fusion(bf16[8,128,2,512]{3,2,1,0:T(2,128)(2,1)S(1)} %reshape.135, f32[8,128,2]{1,2,0:T(2,128)S(1)} %copy.77, f32[8,128,2,128]{3,1,0,2:T(8,128)} %bitcast.63, f32[8,128,2,128]{3,1,0,2:T(8,128)} %bitcast.61), kind=kOutput, calls=%fused_computation.32 | convolution fusion | flops 540016640 | bytes 12591104 | tf_op jit(solution)/shard_map/njhd,njhv->nhdv/dot_general | solution.py:100
  34.7 21.0 %while.27 = (s32[]{:T(128)}, f32[2,256,512]{2,1,0:T(8,128)S(1)}, f32[8,2,256,512]{3,2,1,0:T(8,128)}, f32[8,2]{1,0:T(8,128)S(1)}, f32[8,2,256,512]{3,2,1,0:T(8,128)}, /*index=5*/s32[]{:T(128)}, s32[]{:T(128)}) while((s32[]{:T(128)}, f32[2,256,512]{2,1,0:T(8,128)S(1)}, f32[8,2,256,512]{3,2,1,0:T(8,128)}, f32[8,2]{1,0:T(8,128)S(1)}, ...), condition=%wide.region_4.5_spmd.clone, body=%wide.region_3.4_spmd.clone.sunk | while | flops 1048579 | bytes 5243512 | solution.py:103
  41.0 1.5 bitcast_add_fusion.3
  46.2 1.5 bitcast_add_fusion.3
  54.2 1.5 bitcast_add_fusion.3
  58.0 23.8 %all-reduce = bf16[16]{0:T(256)(128)(2,1)S(1)} all-reduce(bf16[16]{0:T(256)(128)(2,1)S(1)} %dynamic-update-slice), channel_id=2, replica_groups=mesh['sp'=8,'tp'=4] {'sp'}, use_global_device_ids=true, to_apply=%add | all-reduce | flops 16 | bytes 64
  82.0 2.0 copy.64
  84.0 2.1 copy.65
  86.1 6.6 %reshape.151 = f32[8,128,2,512]{3,2,1,0:T(2,128)} reshape(bf16[1024,1024]{1,0:T(8,128)(2,1)} %param.18) | data formatting | bytes 6291456 | tf_op jit(solution)/shard_map/convert_element_type | solution.py:125
  92.6 39.8 %all-gather.13.cloned.1.call-done = bf16[16,256,512]{2,1,0:T(8,128)(2,1)} async-done(((bf16[2,256,512]{2,1,0:T(8,128)(2,1)}), bf16[16,256,512]{2,1,0:T(8,128)(2,1)}) %all-gather.13.cloned.1.call-update) | async-done | bytes 4194320 | tf_op jit(solution)/shard_map/all_gather | solution.py:17
  132.4 12.0 %while.28 = (s32[]{:T(128)}, f32[2,256,512]{2,1,0:T(8,128)S(1)}, s32[]{:T(128)}, bf16[8,2]{1,0:T(8,128)(2,1)S(1)}, bf16[8,2,256,512]{3,2,1,0:T(8,128)(2,1)}, /*index=5*/s32[]{:T(128)}, s32[]{:T(128)}) while((s32[]{:T(128)}, f32[2,256,512]{2,1,0:T(8,128)S(1)}, s32[]{:T(128)}, bf16[8,2]{1,0:T(8,128)(2,1)S(1)}, ...), condition=%wide.region_6.7_spmd.clone, body=%wide.region_5.6_spmd.clone.sunk | while | flops 1310726 | bytes 2621565 | solution.py:34
  144.4 6.8 %fusion.2 = f32[8,2,512,128]{2,3,1,0:T(8,128)} fusion(f32[8,2,256,512]{3,2,1,0:T(8,128)} %get-tuple-element.129, f32[2,256,512]{2,1,0:T(8,128)S(1)} %get-tuple-element.128, f32[8,2]{1,0:T(8,128)S(1)} %copy.76, f32[8,128,2]{1,2,0:T(2,128)S(1)} %copy.81, bf16[8,128,2,128]{3,1,0,2:T(8,128)(2,1)} %bitcast.67, bf16[8,128,2,128]{3,1,0,2:T(8,128)(2,1)} %bitcast.65), kind=kOutput, calls=%fused_computation.9 | convolution fusion | flops 546832384 | bytes 14688320 | tf_op jit(solution)/shard_map/nihd,nhdv->nihv/dot_general | solution.py:118
  151.2 6.2 %multiply_reduce_fusion = (f32[8,128,2]{1,2,0:T(2,128)S(1)}, f32[8,128,2,512]{3,1,2,0:T(8,128)}) fusion(f32[8,2,512,128]{2,3,1,0:T(8,128)} %fusion.2, bf16[8,128,2,512]{3,2,1,0:T(2,128)(2,1)S(1)} %reshape.135, f32[2,8,128]{2,0,1:T(2,128)S(1)} %copy.73, pred[128,128]{1,0:T(8,128)(4,1)S(1)} %iota_compare_fusion, f32[8,128,2,128]{3,1,0,2:T(8,128)} %bitcast.64, ...), kind=kOutput, calls=%fused_computation.12 | convolution fusion | flops 410777600 | bytes 13664256 | tf_op jit(solution)/shard_map/hnij,njhv->nihv/dot_general | solution.py:94
  157.4 4.3 multiply_convert_fusion.1
  161.8 2.6 copy.84
  164.4 9.3 %convolution_convert_fusion.1 = bf16[1024,2048]{1,0:T(8,128)(2,1)} fusion(bf16[1024,2048]{1,0:T(8,128)(2,1)} %param.20, bf16[128,8,8,128]{3,2,1,0:T(8,128)(2,1)} %bitcast.71), kind=kOutput, calls=%fused_computation.16 | convolution fusion | flops 4297064448 | bytes 10485760 | tf_op jit(solution)/shard_map/dot_general | solution.py:143
  175.1 41.9 %reduce-scatter.3.cloned.1.call-done = bf16[256,2048]{1,0:T(8,128)(2,1)} async-done(((bf16[1024,2048]{1,0:T(8,128)(2,1)}), bf16[256,2048]{1,0:T(8,128)(2,1)}) %reduce-scatter.3.cloned.1.call-update) | async-done | bytes 1048592 | tf_op jit(solution)/shard_map/reduce_scatter | solution.py:142
  217.0 1.6 fusion.5
  218.7 2.6 fusion.7
  221.6 122.5 %all-gather.11.cloned.1.call-done = bf16[2048,2048]{1,0:T(8,128)(2,1)} async-done(((bf16[2048,256]{1,0:T(8,128)(2,1)}), bf16[2048,2048]{1,0:T(8,128)(2,1)}) %all-gather.11.cloned.1.call-update) | async-done | bytes 8388624 | tf_op jit(solution)/shard_map/all_gather | solution.py:160
  344.0 124.7 %all-gather.9.cloned.1.call-done = bf16[2048,2048]{1,0:T(8,128)(2,1)} async-done(((bf16[256,2048]{1,0:T(8,128)(2,1)}), bf16[2048,2048]{1,0:T(8,128)(2,1)}) %all-gather.9.cloned.1.call-update) | async-done | bytes 8388624 | tf_op jit(solution)/shard_map/all_gather | solution.py:154
  468.7 34.1 %all-gather.7.cloned.1.call-done = bf16[1024,2048]{1,0:T(8,128)(2,1)} async-done(((bf16[256,2048]{1,0:T(8,128)(2,1)}), bf16[1024,2048]{1,0:T(8,128)(2,1)}) %all-gather.7.cloned.1.call-update) | async-done | bytes 4194320 | tf_op jit(solution)/shard_map/all_gather | solution.py:151
  502.8 25.4 %convolution_convert_fusion = bf16[1024,2048]{1,0:T(8,128)(2,1)} fusion(bf16[2048,2048]{1,0:T(8,128)(2,1)} %all-gather.11.cloned.1.call-done, bf16[1024,2048]{1,0:T(8,128)(2,1)} %all-gather.7.cloned.1.call-done, bf16[2048,2048]{1,0:T(8,128)(2,1)} %all-gather.9.cloned.1.call-done), kind=kOutput, calls=%fused_computation.15 | convolution fusion | flops 17188257792 | bytes 25165824 | tf_op jit(solution)/shard_map/dot_general | solution.py:158
  528.2 44.8 %reduce-scatter.5.cloned.1.call-done = bf16[256,2048]{1,0:T(8,128)(2,1)} async-done(((bf16[1024,2048]{1,0:T(8,128)(2,1)}), bf16[256,2048]{1,0:T(8,128)(2,1)}) %reduce-scatter.5.cloned.1.call-update) | async-done | bytes 1048592 | tf_op jit(solution)/shard_map/reduce_scatter | solution.py:163
  572.9 2.7 fusion.8
  (87 shorter events, 35.7 us)
Async XLA Ops:
  6.5 125.9 %all-gather.13.cloned.1.call-start = ((), (), s32[]{:S(2)}) async-start(), calls=%async_computation.7 | async-start | bytes 4718592 | tf_op jit(solution)/shard_map/all_gather | solution.py:17
  18.5 5.1 copy-start.2
  34.7 22.0 %copy-start.4 = (u32[32]{0:T(128)S(1)}, u32[32]{0:T(128)}, u32[]{:S(2)}) copy-start(u32[32]{0:T(128)} %constant.79) | copy-start | bytes 388
  56.6 160.5 %reduce-scatter.3.cloned.1.call-start = ((), (), s32[]{:S(2)}) async-start(), calls=%async_computation.2 | async-start | bytes 5242880 | tf_op jit(solution)/shard_map/reduce_scatter | solution.py:142
  173.7 1.4 copy-start.3
  173.7 43.3 %copy-start = (bf16[256,2048]{1,0:T(8,128)(2,1)S(1)}, bf16[256,2048]{1,0:T(8,128)(2,1)}, u32[]{:S(2)}) copy-start(bf16[256,2048]{1,0:T(8,128)(2,1)} %param.14) | copy-start | bytes 3145732
  173.8 170.3 %all-gather.11.cloned.1.call-start = ((), (), s32[]{:S(2)}) async-start(), calls=%async_computation.5 | async-start | bytes 9437184 | tf_op jit(solution)/shard_map/all_gather | solution.py:160
  174.5 294.2 %all-gather.9.cloned.1.call-start = ((), (), s32[]{:S(2)}) async-start(), calls=%async_computation.4 | async-start | bytes 9437184 | tf_op jit(solution)/shard_map/all_gather | solution.py:154
  175.1 327.7 %all-gather.7.cloned.1.call-start = ((), (), s32[]{:S(2)}) async-start(), calls=%async_computation.3 | async-start | bytes 5242880 | tf_op jit(solution)/shard_map/all_gather | solution.py:151
  221.3 351.6 %reduce-scatter.5.cloned.1.call-start = ((), (), s32[]{:S(2)}) async-start(), calls=%async_computation.6 | async-start | bytes 5242880 | tf_op jit(solution)/shard_map/reduce_scatter | solution.py:163
  528.2 44.8 %copy-start.1 = (bf16[256,2048]{1,0:T(8,128)(2,1)S(1)}, bf16[256,2048]{1,0:T(8,128)(2,1)}, u32[]{:S(2)}) copy-start(bf16[256,2048]{1,0:T(8,128)(2,1)} %reduce-scatter.3.cloned.1.call-done) | copy-start | bytes 3145732
Sparse Core Ops, SparseCore 0:
  56.7 75.6 all-gather.12
  173.9 43.1 reduce-scatter.2
  219.1 124.9 all-gather.10
  346.0 122.6 all-gather.8
  470.1 32.6 all-gather.6
  528.3 44.5 reduce-scatter.4
where the time goes:
time: 584 us; the launch traced here: 582 us
  waiting for transfers between devices  409 us (70%)
  matrix products  54.3 us (9%)
  other arithmetic  53.1 us (9%)
  local copies, waits for them, and re-layouts  27.3 us (5%)
  blocking collectives  23.8 us (4%)
  between operations  14.2 us (2%)
    all_gather x1, waiting for transfers between devices, body(): lax.all_gather(up_weight, 'sp', axis=0, tiled=True)  125 us
    all_gather x1, waiting for transfers between devices, body(): lax.all_gather(down_weight, 'sp', axis=1, tiled=True)  122 us
    reduce_scatter x1, waiting for transfers between devices, body(): lax.psum_scatter(partial_sums.astype(jnp.bfloat16), 'tp', scatter_dimensi...  44.8 us
    reduce_scatter x1, waiting for transfers between devices, body(): lax.psum_scatter(jnp.dot(gated_out, retention_output_weight, preferred_el...  41.9 us
    all_gather x1, waiting for transfers between devices, carried_in(): lax.all_gather(part.astype(kind), axis)  39.8 us
    all_gather x1, waiting for transfers between devices, body(): lax.all_gather(normalize(updated, norm_gain), 'tp', axis=0, tiled=True)  34.1 us
    dot_general x1, matrix products, body(): jnp.dot(hidden, lax.all_gather(down_weight, 'sp', axis=1, tiled=True), pr...  25.4 us
    unnamed x1, blocking collectives  23.8 us
  transfers between devices with their start and end apart: 6, of which 6 were waited for; matrix products, arithmetic and copies ran while one was open for 3% of the time, Pallas kernels for 0%

commit v1 on v0

v1 whole, which is shorter than its diff:
```python
import functools

import jax
import jax.numpy as jnp
from jax import lax
from jax.experimental import pallas as pl
from jax.experimental.pallas import tpu as pltpu
from jax.sharding import PartitionSpec as P


DK = 256
DV = 512
BLOCK = 128
EPS = 1e-06
BF = jnp.bfloat16
F32 = jnp.float32
TAIL = 16


def params(mib=48):
    return pltpu.CompilerParams(vmem_limit_bytes=mib * 1024 * 1024)


def dot(a, b, contract=((1,), (0,))):
    return lax.dot_general(a, b, (contract, ((), ())), preferred_element_type=F32)


def decay_sums(log_decay):
    blocks = log_decay.shape[0]
    lane = lax.broadcasted_iota(jnp.int32, (blocks, BLOCK), 1)
    row = lax.broadcasted_iota(jnp.int32, (blocks, BLOCK), 0)
    cum = log_decay
    step = 1
    while step < BLOCK:
        cum = cum + jnp.where(lane >= step, pltpu.roll(cum, step, 1), 0.0)
        step *= 2
    total = jnp.broadcast_to(cum[:, BLOCK - 1 :], (blocks, BLOCK))
    upto = total
    step = 1
    while step < blocks:
        upto = upto + jnp.where(row >= step, pltpu.roll(upto, step, 0), 0.0)
        step *= 2
    padded = jnp.concatenate([cum, jnp.zeros((BLOCK - blocks, BLOCK), F32)], axis=0)
    return cum, padded.T, total, upto - total, upto[blocks - 1 :, :]


def turned(part, n, table_ref):
    half = part.shape[1] // 2
    cos_r, sin_r = table_ref[0, :BLOCK, :], table_ref[1, :BLOCK, :]
    cos_b, sin_b = table_ref[0, BLOCK + n : BLOCK + n + 1, :], table_ref[1, BLOCK + n : BLOCK + n + 1, :]
    cosine = cos_r * cos_b - sin_r * sin_b
    sine = sin_r * cos_b + cos_r * sin_b
    first, second = part[:, :half].astype(F32), part[:, half:].astype(F32)
    return first * cosine - second * sine, first * sine + second * cosine


def state_kernel(key_ref, value_ref, decay_ref, table_ref, out_ref, kd_ref, *, halves):
    blocks = decay_ref.shape[1]
    _, col, _, before, whole = decay_sums(decay_ref[0])
    scale = DK ** (-0.5)
    for n in range(blocks):
        rows = pl.ds(n * BLOCK, BLOCK)
        a, b = turned(key_ref[rows, :], n, table_ref)
        a, b = (a * scale).astype(BF).astype(F32), (b * scale).astype(BF).astype(F32)
        factor = jnp.exp(whole - before[n : n + 1, :] - jnp.broadcast_to(col[:, n : n + 1], (BLOCK, BLOCK)))
        kd_ref[rows, : DK // 2] = (a * factor).astype(BF)
        kd_ref[rows, DK // 2 :] = (b * factor).astype(BF)
    state = dot(kd_ref[...], value_ref[...], ((0,), (0,))).astype(BF)
    decay = jnp.broadcast_to(jnp.exp(whole[:, :1]), (TAIL, DV))
    high = decay.astype(BF).astype(F32)
    row = lax.broadcasted_iota(jnp.int32, (TAIL, DV), 0)
    tail = jnp.where(row == 0, high, decay - high).astype(BF)
    size = DK // halves
    for j in range(halves):
        out_ref[j, :size, :] = state[j * size : (j + 1) * size, :]
        out_ref[j, size:, :] = tail


def local_kernel(query_ref, key_ref, value_ref, decay_ref, table_ref, out_ref, qd_ref, state_ref):
    blocks = decay_ref.shape[1]
    cum, col, total, before, _ = decay_sums(decay_ref[0])
    scale = DK ** (-0.5)
    causal = lax.broadcasted_iota(jnp.int32, (BLOCK, BLOCK), 0) >= lax.broadcasted_iota(
        jnp.int32, (BLOCK, BLOCK), 1
    )
    for n in range(blocks):
        rows = pl.ds(n * BLOCK, BLOCK)
        qa, qb = turned(query_ref[rows, :], n, table_ref)
        ka, kb = turned(key_ref[rows, :], n, table_ref)
        qa, qb = qa.astype(BF), qb.astype(BF)
        ka, kb = (ka * scale).astype(BF), (kb * scale).astype(BF)
        query = jnp.concatenate([qa, qb], axis=1)
        key = jnp.concatenate([ka, kb], axis=1)
        value = value_ref[rows, :]
        down = jnp.broadcast_to(col[:, n : n + 1], (BLOCK, BLOCK))
        spread = down - cum[n : n + 1, :]
        factor = jnp.where(causal, jnp.exp(jnp.minimum(spread, 0.0)), 0.0)
        weights = (dot(query, key, ((1,), (1,))) * factor).astype(BF)
        result = dot(weights, value)
        from_block = jnp.exp(down)
        if n:
            near = jnp.concatenate(
                [(qa.astype(F32) * from_block).astype(BF), (qb.astype(F32) * from_block).astype(BF)], axis=1
            )
            result = result + dot(near, state_ref[...].astype(BF))
        out_ref[rows, :] = result
        from_start = jnp.exp(down + before[n : n + 1, :])
        qd_ref[rows, : DK // 2] = (qa.astype(F32) * from_start).astype(BF)
        qd_ref[rows, DK // 2 :] = (qb.astype(F32) * from_start).astype(BF)
        if n + 1 < blocks:
            to_end = jnp.exp(total[n : n + 1, :] - down)
            kd = jnp.concatenate(
                [(ka.astype(F32) * to_end).astype(BF), (kb.astype(F32) * to_end).astype(BF)], axis=1
            )
            term = dot(kd, value, ((0,), (0,)))
            if n:
                state_ref[...] = jnp.exp(total[n : n + 1, :1]) * state_ref[...] + term
            else:
                state_ref[...] = term


def gate_kernel(order_ref, local_ref, qd_ref, in_ref, gate_ref, weight_ref, out_ref, gated_ref):
    heads = local_ref.shape[1] // DV
    for h in range(heads):
        cols = pl.ds(h * DV, DV)
        retained = local_ref[:, cols] + dot(qd_ref[:, pl.ds(h * DK, DK)], in_ref[h])
        mean = jnp.mean(retained * retained, axis=-1, keepdims=True)
        gate = gate_ref[:, cols].astype(F32)
        silu = gate / (1.0 + jnp.exp(-gate))
        gated_ref[:, cols] = (silu * (retained * lax.rsqrt(mean + EPS))).astype(BF)
    out_ref[0] = dot(gated_ref[...], weight_ref[...]).astype(BF)


def norm_kernel(y_ref, resid_ref, a_ref, b_ref, *rest, regions):
    far, (gain_ref, updated_ref, normed_ref) = rest[:-3], rest[-3:]
    mixed = a_ref[...].astype(F32) + b_ref[...].astype(F32)
    for ref in far:
        mixed = mixed + ref[...].astype(F32)
    updated = (resid_ref[...].astype(F32) + mixed).astype(BF)
    updated_ref[...] = updated
    wide = updated.astype(F32)
    scaled = wide * lax.rsqrt(jnp.mean(wide * wide, axis=-1, keepdims=True) + EPS)
    normed = (scaled * gain_ref[...].astype(F32)).astype(BF)
    size = normed.shape[1] // regions
    half = regions // 2
    lower = y_ref[0] == 0
    for r in range(half):
        even = normed[:, 2 * r * size : (2 * r + 1) * size]
        odd = normed[:, (2 * r + 1) * size : (2 * r + 2) * size]
        normed_ref[:, r * size : (r + 1) * size] = jnp.where(lower, even, odd)
        normed_ref[:, (half + r) * size : (half + r + 1) * size] = jnp.where(lower, odd, even)


def last_kernel(y_ref, updated_ref, *rest, regions):
    left_ref, right_ref, out_ref = rest
    size = 2 * left_ref.shape[1] // regions
    half = regions // 2
    lower = y_ref[0] == 0
    for r in range(half):
        own = left_ref[:, r * size : (r + 1) * size]
        other = right_ref[:, r * size : (r + 1) * size]
        even, odd = pl.ds(2 * r * size, size), pl.ds((2 * r + 1) * size, size)
        out_ref[:, even] = (updated_ref[:, even].astype(F32) + jnp.where(lower, own, other)).astype(BF)
        out_ref[:, odd] = (updated_ref[:, odd].astype(F32) + jnp.where(lower, other, own)).astype(BF)


def region_offsets(z_ref, planes, size, sides):
    offsets = []
    for side in range(sides):
        for s in range(planes):
            plane = lax.rem(z_ref[0] + (planes - s), planes)
            offsets.append(pl.multiple_of((side * planes + plane) * size, size))
    return offsets


def up_kernel(z_ref, *rest, planes, sources):
    rows, up, hidden_ref = rest[:sources], rest[sources:-1], rest[-1]
    size, units = up[0].shape
    offsets = region_offsets(z_ref, planes, size, 2)
    chunk = min(256, units)
    start = 0
    for ref in rows:
        place = pl.ds(start, ref.shape[0])
        start += ref.shape[0]
        for c in range(units // chunk):
            cols = pl.ds(c * chunk, chunk)
            acc = dot(ref[:, pl.ds(offsets[0], size)], up[0][:, cols])
            for j in range(1, len(up)):
                acc = acc + dot(ref[:, pl.ds(offsets[j], size)], up[j][:, cols])
            positive = jnp.maximum(acc, 0.0)
            hidden_ref[place, cols] = (positive * positive).astype(BF)


def down_kernel(z_ref, *rest, planes):
    hidden, down, (mine_ref, other_ref) = rest[: -2 - planes], rest[-2 - planes : -2], rest[-2:]
    offsets = region_offsets(z_ref, planes, down[0].shape[1], 1)
    half = hidden[0].shape[0] // 2
    for i, ref in enumerate(hidden):
        place = pl.ds(i * half, half)
        for j, piece in enumerate(down):
            cols = pl.ds(offsets[j], piece.shape[1])
            product = dot(ref[...], piece[...]).astype(BF)
            mine_ref[place, cols] = product[:half]
            other_ref[place, cols] = product[half:]


def make_body(n_sp, n_tp):
    n_x, n_z = n_tp // 2, n_sp // 2

    def over_tp(value, turn):
        return lax.ppermute(value, "tp", [(t, turn(t)) for t in range(n_tp)])

    def over_sp(value, pairs):
        return lax.ppermute(value, "sp", pairs)

    def swap_core(value):
        return over_tp(value, lambda t: t ^ 1)

    def shift_x(value, s):
        return over_tp(value, lambda t: (t + 2 * s) % n_tp)

    def swap_y(value):
        return over_sp(value, [(i, i ^ 1) for i in range(n_sp)])

    def shift_z(value, s):
        return over_sp(value, [(i, (i + 2 * s) % n_sp) for i in range(n_sp)])

    def forward_z(value, s):
        return over_sp(value, [(i, i + 2 * s) for i in range(n_sp - 2 * s)])

    def swap_z(value):
        return over_sp(value, [(i, i ^ 2) for i in range(n_sp)])

    def body(resid, queries, keys, values, gates, log_decay, out_weight, gain, up_weight, down_weight):
        sp, tp = lax.axis_index("sp"), lax.axis_index("tp")
        y, z, core, x = sp % 2, sp // 2, tp % 2, tp // 2
        rows, heads = queries.shape[0], log_decay.shape[0]
        own_rows, width = resid.shape
        blocks = rows // BLOCK

        units = up_weight.shape[1] // 2
        same, other = (z % 2) * units, (1 - z % 2) * units
        up_same = lax.dynamic_slice_in_dim(up_weight, same, units, 1)
        up_other = lax.dynamic_slice_in_dim(up_weight, other, units, 1)
        down_same = lax.dynamic_slice_in_dim(down_weight, same, units, 0)
        down_other = lax.dynamic_slice_in_dim(down_weight, other, units, 0)
        up = [up_same] + [shift_z(up_other if s % 2 else up_same, s) for s in range(1, n_z)]
        down = [down_same] + [shift_z(down_other if s % 2 else down_same, s) for s in range(1, n_z)]
        up = up + [swap_y(piece) for piece in up]
        down = down + [swap_y(piece) for piece in down]

        inverse = 10000.0 ** (-jnp.arange(0, DK, 2, dtype=F32) / DK)
        places = jnp.concatenate(
            [jnp.arange(BLOCK, dtype=jnp.int32), sp * rows + BLOCK * jnp.arange(blocks, dtype=jnp.int32)]
        )
        angles = places[:, None].astype(F32) * inverse[None, :]
        table = jnp.stack([jnp.cos(angles), jnp.sin(angles)])
        decay = log_decay.reshape(heads, blocks, BLOCK)
        halves = 2 // heads
        size = DK // halves
        table_spec = pl.BlockSpec(table.shape, lambda h: (0, 0, 0))
        decay_spec = pl.BlockSpec((1, blocks, BLOCK), lambda h: (h, 0, 0))
        key_spec = pl.BlockSpec((rows, DK), lambda h: (0, h))
        value_spec = pl.BlockSpec((rows, DV), lambda h: (0, h))
        own_state = pl.pallas_call(
            functools.partial(state_kernel, halves=halves),
            out_shape=jax.ShapeDtypeStruct((2, size + TAIL, DV), BF),
            grid=(heads,),
            in_specs=[key_spec, value_spec, decay_spec, table_spec],
            out_specs=pl.BlockSpec((halves, size + TAIL, DV), lambda h: (h, 0, 0)),
            scratch_shapes=[pltpu.VMEM((rows, DK), BF)],
            compiler_params=params(),
            name="state",
        )(keys, values, decay, table)

        local, query_decayed = pl.pallas_call(
            local_kernel,
            out_shape=(
                jax.ShapeDtypeStruct((rows, heads * DV), F32),
                jax.ShapeDtypeStruct((rows, heads * DK), BF),
            ),
            grid=(heads,),
            in_specs=[key_spec, key_spec, value_spec, decay_spec, table_spec],
            out_specs=(value_spec, key_spec),
            scratch_shapes=[pltpu.VMEM((DK, DV), F32)],
            compiler_params=params(),
            name="local",
        )(queries, keys, values, decay, table)

        def parts(payload):
            wide = payload.astype(F32)
            return wide[size, 0] + wide[size + 1, 0], wide[:size]

        def pick(pair, index):
            return lax.dynamic_index_in_dim(pair, index, 0, keepdims=False)

        got = swap_y(pick(own_state, 1 - y))
        mine = pick(own_state, y)
        first = jnp.where(y == 0, mine, got)
        second = jnp.where(y == 0, got, mine)
        (first_decay, first_state), (second_decay, second_state) = parts(first), parts(second)
        plane_decay = first_decay * second_decay
        plane_state = second_decay * first_state + second_state
        row = lax.broadcasted_iota(jnp.int32, (TAIL, DV), 0)
        before_decay, before = jnp.ones((), F32), jnp.zeros((size, DV), F32)
        reach = 1
        while reach < n_z:
            upto_decay = before_decay * plane_decay
            upto = plane_decay * before + plane_state
            high = upto_decay.astype(BF).astype(F32)
            tail = jnp.where(row == 0, high, upto_decay - high)
            sent = forward_z(jnp.concatenate([upto, tail], axis=0).astype(BF), reach)
            far_decay, far_state = parts(sent)
            before = before_decay * far_state + before
            before_decay = before_decay * far_decay
            reach *= 2
        after_first = (first_decay * before + first_state).astype(BF)
        before = before.astype(BF)
        sent = swap_y(jnp.where(y == 0, after_first, before))
        kept = jnp.where(y == 0, before, after_first)
        incoming = jnp.stack([jnp.where(y == 0, kept, sent), jnp.where(y == 0, sent, kept)])
        incoming = incoming.reshape(heads, DK, DV)

        def projected(order):
            count = order.shape[0]
            return pl.pallas_call(
                gate_kernel,
                out_shape=jax.ShapeDtypeStruct((count, own_rows, width), BF),
                grid_spec=pltpu.PrefetchScalarGridSpec(
                    num_scalar_prefetch=1,
                    grid=(count,),
                    in_specs=[
                        pl.BlockSpec((own_rows, heads * DV), lambda j, o: (o[j], 0)),
                        pl.BlockSpec((own_rows, heads * DK), lambda j, o: (o[j], 0)),
                        pl.BlockSpec((heads, DK, DV), lambda j, o: (0, 0, 0)),
                        pl.BlockSpec((own_rows, heads * DV), lambda j, o: (o[j], 0)),
                        pl.BlockSpec(out_weight.shape, lambda j, o: (0, 0)),
                    ],
                    out_specs=pl.BlockSpec((1, own_rows, width), lambda j, o: (j, 0, 0)),
                    scratch_shapes=[pltpu.VMEM((own_rows, heads * DV), BF)],
                ),
                compiler_params=params(),
            )(order, local, query_decayed, incoming, gates, out_weight)

        def places_of(steps):
            chips = [2 * ((x + s) % n_x) for s in steps]
            return jnp.stack([c + 1 - core for c in chips] + [c + core for c in chips]).astype(jnp.int32)

        far = projected(places_of(range(1, n_x)))
        near = projected(places_of([0]))
        far_sum = (swap_core(far[: n_x - 1]).astype(F32) + far[n_x - 1 :].astype(F32)).astype(BF)
        arrived = [shift_x(far_sum[s - 1], s) for s in range(1, n_x)]
        near_other = swap_core(near[0])

        steps = max(own_rows // 128, 1)
        tall = own_rows // steps
        row_spec = pl.BlockSpec((tall, width), lambda i, o: (i, 0))
        y_word = y.astype(jnp.int32).reshape(1)
        updated, normed = pl.pallas_call(
            functools.partial(norm_kernel, regions=n_sp),
            out_shape=(jax.ShapeDtypeStruct(resid.shape, BF), jax.ShapeDtypeStruct(resid.shape, BF)),
            grid_spec=pltpu.PrefetchScalarGridSpec(
                num_scalar_prefetch=1,
                grid=(steps,),
                in_specs=[row_spec] * (3 + n_x - 1) + [pl.BlockSpec((1, width), lambda i, o: (0, 0))],
                out_specs=(row_spec, row_spec),
            ),
            compiler_params=params(),
            name="norm",
        )(y_word, resid, near[1], near_other, *arrived, gain.reshape(1, width))

        z_word = z.astype(jnp.int32).reshape(1)

        def raised(sources):
            args = (z_word, *sources, *up)
            return pl.pallas_call(
                functools.partial(up_kernel, planes=n_z, sources=len(sources)),
                out_shape=jax.ShapeDtypeStruct((2 * own_rows, units), BF),
                in_specs=[pl.BlockSpec(memory_space=pltpu.SMEM)]
                + [pl.BlockSpec(memory_space=pltpu.VMEM)] * (len(args) - 1),
                out_specs=pl.BlockSpec(memory_space=pltpu.VMEM),
                compiler_params=params(),
                name="up",
            )(*args)

        def lowered(sources, side):
            args = (z_word, *sources, *down[side * n_z : (side + 1) * n_z])
            tall = len(sources) * own_rows
            mine, others = pl.pallas_call(
                functools.partial(down_kernel, planes=n_z),
                out_shape=(jax.ShapeDtypeStruct((tall, width // 2), BF),) * 2,
                in_specs=[pl.BlockSpec(memory_space=pltpu.SMEM)]
                + [pl.BlockSpec(memory_space=pltpu.VMEM)] * (len(args) - 1),
                out_specs=(pl.BlockSpec(memory_space=pltpu.VMEM),) * 2,
                compiler_params=params(),
                name="down",
            )(*args)
            others = swap_core(others)
            parts = [slice(i * own_rows, (i + 1) * own_rows) for i in range(len(sources))]
            sums = [mine[part].astype(F32) + others[part].astype(F32) for part in parts]
            return lax.optimization_barrier(tuple(sums))

        near_x = range(1, n_x)
        top = own_rows // 2
        from_x = {s: shift_x(normed, s) for s in near_x}
        from_z = swap_z(normed)
        corner = {s: [shift_x(from_z[:top], s), swap_z(from_x[s][top:])] for s in near_x}
        chunks = {"o": [normed], "z": [from_z]}
        for s in near_x:
            chunks[f"x{s}"] = [from_x[s]]
            chunks[f"c{s}"] = corner[s]
        hidden = {key: raised(parts + [swap_core(part) for part in parts]) for key, parts in chunks.items()}
        straight = [hidden[f"x{s}"] for s in near_x] + [hidden["z"], hidden["o"]]
        corners = [hidden[f"c{s}"] for s in near_x]

        def home(value, s):
            return shift_x(value.astype(BF), n_x - s).astype(F32)

        *left_x, left_z, left_sum = lowered(straight, 0)
        left_c = lowered(corners, 0)
        *right_x, right_z, right_sum = lowered(straight, 1)
        right_c = lowered(corners, 1)
        for s in near_x:
            left_sum = left_sum + home(left_x[s - 1], s)
            left_z = left_z + home(left_c[s - 1], s)
        right_sum = right_sum + swap_z(right_z.astype(BF)).astype(F32)
        right_x = [right_x[s - 1] + swap_z(right_c[s - 1].astype(BF)).astype(F32) for s in near_x]
        left_sum = left_sum + swap_z(left_z.astype(BF)).astype(F32)
        for s in near_x:
            right_sum = right_sum + home(right_x[s - 1], s)
        pieces = [left_sum, right_sum]

        return pl.pallas_call(
            functools.partial(last_kernel, regions=n_sp),
            out_shape=jax.ShapeDtypeStruct(resid.shape, BF),
            grid_spec=pltpu.PrefetchScalarGridSpec(
                num_scalar_prefetch=1,
                grid=(steps,),
                in_specs=[row_spec] + [pl.BlockSpec((tall, width // 2), lambda i, o: (i, 0))] * 2,
                out_specs=row_spec,
            ),
            compiler_params=params(),
            name="last",
        )(y_word, updated, *pieces)

    return body


def solution(mesh):
    placed = (
        P(("sp", "tp"), None),
        P("sp", "tp"),
        P("sp", "tp"),
        P("sp", "tp"),
        P("sp", "tp"),
        P("tp", "sp"),
        P("tp", None),
        P(),
        P("sp", "tp"),
        P("tp", "sp"),
    )
    n_sp, n_tp = mesh.shape["sp"], mesh.shape["tp"]
    body = make_body(n_sp, n_tp)

    return jax.shard_map(body, mesh=mesh, in_specs=placed, out_specs=P(("sp", "tp"), None), check_vma=False)
```

time: 584 us -> 319 us (0.55)
  waiting for transfers between devices: 409 us -> 181 us
  starting transfers between devices: 0.42 us -> 56.6 us
  Pallas kernels: 0 us -> 55.7 us
  matrix products: 54.3 us -> 0 us
  other arithmetic: 53.1 us -> 8.01 us
  blocking collectives: 23.8 us -> 0 us
  local copies, waits for them, and re-layouts: 27.3 us -> 13.5 us
  between operations: 14.2 us -> 4.31 us
    all_gather x4 -> x0, waiting for transfers between devices: 321 us -> none  [the longest x1 125 us: body(): lax.all_gather(up_weight, 'sp', axis=0, tiled=True)]
    ppermute x0 -> x40, waiting for transfers between devices: none -> 181 us  [the longest x23 169 us: over_sp(): return lax.ppermute(value, 'sp', pairs)]
    reduce_scatter x2 -> x0, waiting for transfers between devices: 86.6 us -> none  [the longest x1 44.8 us: body(): lax.psum_scatter(partial_sums.astype(jnp.bfloat16), 'tp', scatter_dimensi...]
    ppermute x0 -> x40, starting transfers between devices: none -> 56.6 us  [the longest x23 48.6 us: over_sp(): return lax.ppermute(value, 'sp', pairs)]
    pallas_call x0 -> x14, Pallas kernels: none -> 55.7 us  [the longest x4 16.2 us: raised(): pl.pallas_call(functools.partial(up_kernel, planes=n_z, sources=len(sourc...]
    dot_general x5 -> x0, matrix products: 54.3 us -> none  [the longest x1 25.4 us: body(): jnp.dot(hidden, lax.all_gather(down_weight, 'sp', axis=1, tiled=True), pr...]
    unnamed x1 -> x0, blocking collectives: 23.8 us -> none
    convert_element_type x17 -> x5, other arithmetic: 13.5 us -> 0.46 us  [the longest x1 0.17 us: body(): left_sum = left_sum + swap_z(left_z.astype(BF)).astype(F32)]
  transfers between devices with their start and end apart: 6 -> 40, of which waited for: 6 -> 16; matrix products, arithmetic and copies ran while one was open for 3% -> 2% of each run, Pallas kernels for 0% -> 14%
where the time goes in v1:
time: 319 us
  waiting for transfers between devices  181 us (57%)
  starting transfers between devices  56.6 us (18%)
  Pallas kernels  55.7 us (17%)
  local copies, waits for them, and re-layouts  13.5 us (4%)
  other arithmetic  8.01 us (3%)
  between operations  4.31 us (1%)
    ppermute x23, waiting for transfers between devices, over_sp(): return lax.ppermute(value, 'sp', pairs)  169 us
    ppermute x23, starting transfers between devices, over_sp(): return lax.ppermute(value, 'sp', pairs)  48.6 us
    pallas_call x4, Pallas kernels, raised(): pl.pallas_call(functools.partial(up_kernel, planes=n_z, sources=len(sourc...  16.2 us
    pallas_call x2, Pallas kernels, projected(): pl.pallas_call(gate_kernel, out_shape=jax.ShapeDtypeStruct((count, own_ro...  12.8 us
    pallas_call x4, Pallas kernels, lowered(): pl.pallas_call(functools.partial(down_kernel, planes=n_z), out_shape=(jax...  12.8 us
    ppermute x17, waiting for transfers between devices, over_tp(): return lax.ppermute(value, 'tp', [(t, turn(t)) for t in range(n_tp)])  11.6 us
    unnamed x51, local copies, waits for them, and re-layouts  9.48 us
    ppermute x17, starting transfers between devices, over_tp(): return lax.ppermute(value, 'tp', [(t, turn(t)) for t in range(n_tp)])  8.02 us
  transfers between devices with their start and end apart: 40, of which 16 were waited for; matrix products, arithmetic and copies ran while one was open for 2% of the time, Pallas kernels for 14%

profile of v1, /device:TPU:0, one launch (start us, length us, event | category | flops | bytes accessed | tf_op | source)
XLA Modules:
  0.0 318.8 jit_solution(14099654547675844186)
XLA Ops:
  3.9 3.2 %state.1 = bf16[2,272,512]{2,1,0:T(8,128)(2,1)S(1)} custom-call(bf16[1024,512]{1,0:T(8,128)(2,1)S(1)} %copy-done.6, bf16[1024,1024]{1,0:T(8,128)(2,1)S(1)} %copy-done.2, f32[2,8,128]{2,1,0:T(8,128)S(1)} %bitcast.32, f32[2,136,128]{2,1,0:T(8,128)S(1)} %pad_maximum_fusion.3.table_ref), custom_call_target="tpu_custom_call" | custom-call | tf_op jit(solution)/shard_map/state/pallas_call | solution.py:265
  7.1 3.1 collective-permute-start
  10.2 6.6 %collective-permute-done = bf16[272,512]{1,0:T(8,128)(2,1)S(1)} collective-permute-done((bf16[272,512]{1,0:T(8,128)(2,1)S(1)}, bf16[272,512]{1,0:T(8,128)(2,1)S(1)}, u32[]{:S(2)}, u32[]{:S(2)}) %collective-permute-start) | collective-permute-done | bytes 278560 | tf_op jit(solution)/shard_map/ppermute | solution.py:214
  20.4 3.7 %collective-permute-start.1 = (bf16[272,512]{1,0:T(8,128)(2,1)S(1)}, bf16[272,512]{1,0:T(8,128)(2,1)S(1)}, u32[]{:S(2)}, u32[]{:S(2)}) collective-permute-start(bf16[272,512]{1,0:T(8,128)(2,1)S(1)} %pad_maximum_fusion.1), channel_id=1, source_target_pairs={{0,8},{4,12},{8,16},{12,20},{16,24},{20,28},{1,9},{5,13},{9,17},{1... | collective-permute-start | bytes 835592 | tf_op jit(solution)/shard_map/ppermute | solution.py:214
  24.1 5.0 %collective-permute-done.1 = bf16[272,512]{1,0:T(8,128)(2,1)S(1)} collective-permute-done((bf16[272,512]{1,0:T(8,128)(2,1)S(1)}, bf16[272,512]{1,0:T(8,128)(2,1)S(1)}, u32[]{:S(2)}, u32[]{:S(2)}) %collective-permute-start.1) | collective-permute-done | bytes 278560 | tf_op jit(solution)/shard_map/ppermute | solution.py:214
  31.4 5.5 %collective-permute-start.2 = (bf16[272,512]{1,0:T(8,128)(2,1)S(1)}, bf16[272,512]{1,0:T(8,128)(2,1)S(1)}, u32[]{:S(2)}, u32[]{:S(2)}) collective-permute-start(bf16[272,512]{1,0:T(8,128)(2,1)S(1)} %pad_maximum_fusion.2), channel_id=1, source_target_pairs={{0,16},{4,20},{8,24},{12,28},{1,17},{5,21},{9,25},{13,29},{2,18},{... | collective-permute-start | bytes 835592 | tf_op jit(solution)/shard_map/ppermute | solution.py:214
  37.0 4.2 %collective-permute-done.2 = bf16[272,512]{1,0:T(8,128)(2,1)S(1)} collective-permute-done((bf16[272,512]{1,0:T(8,128)(2,1)S(1)}, bf16[272,512]{1,0:T(8,128)(2,1)S(1)}, u32[]{:S(2)}, u32[]{:S(2)}) %collective-permute-start.2) | collective-permute-done | bytes 278560 | tf_op jit(solution)/shard_map/ppermute | solution.py:214
  41.2 2.1 broadcast_select_fusion
  46.0 7.6 %local.1 = (f32[1024,1024]{1,0:T(8,128)}, bf16[1024,512]{1,0:T(8,128)(2,1)S(1)}) custom-call(bf16[1024,512]{1,0:T(8,128)(2,1)S(1)} %copy-done.11, bf16[1024,512]{1,0:T(8,128)(2,1)S(1)} %copy-done.7, bf16[1024,1024]{1,0:T(8,128)(2,1)S(1)} %copy-done.3, f32[2,8,128]{2,1,0:T(8,128)S(1)} %bitcast.33, f32[2,136,128]{2,1,0:T(8,128)S(1)} %pad_maximum_fusion.3.table_ref), custom_call_target="tpu_custom_call" | custom-call | tf_op jit(solution)/shard_map/local/pallas_call | solution.py:276
  55.3 6.4 %shard_map.101 = bf16[2,256,2048]{2,1,0:T(8,128)(2,1)S(1)} custom-call(s32[2]{0:T(128)S(1)} %get-tuple-element.67.order_ref, f32[1024,1024]{1,0:T(8,128)} %get-tuple-element.23.local_ref, bf16[1024,512]{1,0:T(8,128)(2,1)S(1)} %get-tuple-element.24.qd_ref, bf16[2,256,512]{2,1,0:T(8,128)(2,1)S(1)} %pad_maximum_fusion.in_ref, bf16[1024,1024]{1,0:T(8,128)(2,1)S(1)} %copy-done.4, ...), custom_call_target="tpu_custom_call" | custom-call | tf_op jit(solution)/shard_map/pallas_call | solution.py:326
  61.8 6.4 %shard_map.100 = bf16[2,256,2048]{2,1,0:T(8,128)(2,1)S(1)} custom-call(s32[2]{0:T(128)S(1)} %get-tuple-element.66.order_ref, f32[1024,1024]{1,0:T(8,128)} %get-tuple-element.23.local_ref, bf16[1024,512]{1,0:T(8,128)(2,1)S(1)} %get-tuple-element.24.qd_ref, bf16[2,256,512]{2,1,0:T(8,128)(2,1)S(1)} %pad_maximum_fusion.in_ref, bf16[1024,1024]{1,0:T(8,128)(2,1)S(1)} %copy-done.4, ...), custom_call_target="tpu_custom_call" | custom-call | tf_op jit(solution)/shard_map/pallas_call | solution.py:326
  74.1 7.4 %collective-permute-start.9 = (bf16[256,1024]{1,0:T(8,128)(2,1)S(1)}, bf16[256,1024]{1,0:T(8,128)(2,1)S(1)}, u32[]{:S(2)}, u32[]{:S(2)}) collective-permute-start(bf16[256,1024]{1,0:T(8,128)(2,1)S(1)} %get-tuple-element.52), channel_id=1, source_target_pairs={{0,8},{4,12},{8,16},{12,20},{16,24},{20,28},{24,0},{28,4},{1,9},{5... | collective-permute-start | bytes 1572872 | tf_op jit(solution)/shard_map/ppermute | solution.py:214
  81.5 2.9 collective-permute-start.11
  85.0 12.2 %collective-permute-done.9.rest_3_.rest_5_ = bf16[256,1024]{1,0:T(8,128)(2,1)S(1)} collective-permute-done((bf16[256,1024]{1,0:T(8,128)(2,1)S(1)}, bf16[256,1024]{1,0:T(8,128)(2,1)S(1)}, u32[]{:S(2)}, u32[]{:S(2)}) %collective-permute-start.9) | collective-permute-done | bytes 524320 | tf_op jit(solution)/shard_map/ppermute | solution.py:214
  98.7 13.8 %collective-permute-start.20 = (bf16[1024,256]{1,0:T(8,128)(2,1)S(1)}, bf16[1024,256]{1,0:T(8,128)(2,1)S(1)}, u32[]{:S(2)}, u32[]{:S(2)}) collective-permute-start(bf16[1024,256]{1,0:T(8,128)(2,1)S(1)} %get-tuple-element.51.rest_3_.rest_1_), channel_id=1, source_target_pairs={{0,16},{4,20},{8,24},{12,28},{16,0},{20,4},{24,8},{28,12},{1,17},{... | collective-permute-start | bytes 1572872 | tf_op jit(solution)/shard_map/ppermute | solution.py:214
  113.7 2.0 norm.1
  115.8 36.6 %collective-permute-done.10.rest_4_.rest_6_ = bf16[256,1024]{1,0:T(8,128)(2,1)S(1)} collective-permute-done((bf16[256,1024]{1,0:T(8,128)(2,1)S(1)}, bf16[256,1024]{1,0:T(8,128)(2,1)S(1)}, u32[]{:S(2)}, u32[]{:S(2)}) %collective-permute-start.10) | collective-permute-done | bytes 524320 | tf_op jit(solution)/shard_map/ppermute | solution.py:214
  154.5 9.2 %collective-permute-done.20.rest_5_.rest_3_ = bf16[1024,256]{1,0:T(8,128)(2,1)S(1)} collective-permute-done((bf16[1024,256]{1,0:T(8,128)(2,1)S(1)}, bf16[1024,256]{1,0:T(8,128)(2,1)S(1)}, u32[]{:S(2)}, u32[]{:S(2)}) %collective-permute-start.20) | collective-permute-done | bytes 524320 | tf_op jit(solution)/shard_map/ppermute | solution.py:214
  164.2 33.0 %collective-permute-done.21.rest_6_.rest_4_ = bf16[1024,256]{1,0:T(8,128)(2,1)S(1)} collective-permute-done((bf16[1024,256]{1,0:T(8,128)(2,1)S(1)}, bf16[1024,256]{1,0:T(8,128)(2,1)S(1)}, u32[]{:S(2)}, u32[]{:S(2)}) %collective-permute-start.21) | collective-permute-done | bytes 524320 | tf_op jit(solution)/shard_map/ppermute | solution.py:214
  199.9 12.1 %collective-permute-done.14.rest_8_.rest_10_ = bf16[256,1024]{1,0:T(8,128)(2,1)S(1)} collective-permute-done((bf16[256,1024]{1,0:T(8,128)(2,1)S(1)}, bf16[256,1024]{1,0:T(8,128)(2,1)S(1)}, u32[]{:S(2)}, u32[]{:S(2)}) %collective-permute-start.14) | collective-permute-done | bytes 524320 | tf_op jit(solution)/shard_map/ppermute | solution.py:214
  212.7 10.2 %collective-permute-done.15.rest_9_.rest_11_ = bf16[256,1024]{1,0:T(8,128)(2,1)S(1)} collective-permute-done((bf16[256,1024]{1,0:T(8,128)(2,1)S(1)}, bf16[256,1024]{1,0:T(8,128)(2,1)S(1)}, u32[]{:S(2)}, u32[]{:S(2)}) %collective-permute-start.15) | collective-permute-done | bytes 524320 | tf_op jit(solution)/shard_map/ppermute | solution.py:214
  225.6 10.7 %collective-permute-done.25.rest_1_ = bf16[128,2048]{1,0:T(8,128)(2,1)S(1)} collective-permute-done((bf16[128,2048]{1,0:T(8,128)(2,1)S(1)}, bf16[128,2048]{1,0:T(8,128)(2,1)S(1)}, u32[]{:S(2)}, u32[]{:S(2)}) %collective-permute-start.25) | collective-permute-done | bytes 524320 | tf_op jit(solution)/shard_map/ppermute | solution.py:214
  238.2 3.9 %up.6.rest_2_ = bf16[512,1024]{1,0:T(8,128)(2,1)S(1)} custom-call(s32[1]{0:T(128)} %bitcast.15.z_ref, bf16[256,2048]{1,0:T(8,128)(2,1)} %copy-done.12, bf16[256,2048]{1,0:T(8,128)(2,1)} %copy-done.21, bf16[256,1024]{1,0:T(8,128)(2,1)S(1)} %get-tuple-element.53.rest_2_.rest_4_, bf16[256,1024]{1,0:T(8,128)(2,1)S(1)} %collective-permute-done.9.rest_3_.rest_5_, ...), custom_call_target="tpu_custom_call" | custom-call | tf_op jit(solution)/shard_map/up/pallas_call | solution.py:376
  242.2 3.9 %up.5.rest_1_ = bf16[512,1024]{1,0:T(8,128)(2,1)S(1)} custom-call(s32[1]{0:T(128)} %bitcast.15.z_ref, bf16[256,2048]{1,0:T(8,128)(2,1)} %copy-done.14, bf16[256,2048]{1,0:T(8,128)(2,1)} %copy-done.22, bf16[256,1024]{1,0:T(8,128)(2,1)S(1)} %get-tuple-element.53.rest_2_.rest_4_, bf16[256,1024]{1,0:T(8,128)(2,1)S(1)} %collective-permute-done.9.rest_3_.rest_5_, ...), custom_call_target="tpu_custom_call" | custom-call | tf_op jit(solution)/shard_map/up/pallas_call | solution.py:376
  246.1 3.9 %up.4.rest_0_ = bf16[512,1024]{1,0:T(8,128)(2,1)S(1)} custom-call(s32[1]{0:T(128)} %bitcast.15.z_ref, bf16[256,2048]{1,0:T(8,128)(2,1)} %copy-done.15, bf16[256,2048]{1,0:T(8,128)(2,1)} %copy-done.23, bf16[256,1024]{1,0:T(8,128)(2,1)S(1)} %get-tuple-element.53.rest_2_.rest_4_, bf16[256,1024]{1,0:T(8,128)(2,1)S(1)} %collective-permute-done.9.rest_3_.rest_5_, ...), custom_call_target="tpu_custom_call" | custom-call | tf_op jit(solution)/shard_map/up/pallas_call | solution.py:376
  250.1 8.8 %collective-permute-done.34.rest_6_.rest_4_ = bf16[1024,256]{1,0:T(8,128)(2,1)S(1)} collective-permute-done((bf16[1024,256]{1,0:T(8,128)(2,1)S(1)}, bf16[1024,256]{1,0:T(8,128)(2,1)S(1)}, u32[]{:S(2)}, u32[]{:S(2)}) %collective-permute-start.34) | collective-permute-done | bytes 524320 | tf_op jit(solution)/shard_map/ppermute | solution.py:214
  258.9 5.0 %down.6 = (bf16[768,1024]{1,0:T(8,128)(2,1)}, bf16[768,1024]{1,0:T(8,128)(2,1)}) custom-call(s32[1]{0:T(128)} %bitcast.15.z_ref, bf16[512,1024]{1,0:T(8,128)(2,1)S(1)} %up.4.rest_0_, bf16[512,1024]{1,0:T(8,128)(2,1)S(1)} %up.5.rest_1_, bf16[512,1024]{1,0:T(8,128)(2,1)S(1)} %up.6.rest_2_, bf16[1024,256]{1,0:T(8,128)(2,1)S(1)} %collective-permute-done.31.rest_3_.rest_1_, ...), custom_call_target="tpu_custom_call" | custom-call | tf_op jit(solution)/shard_map/down/pallas_call | solution.py:389
  263.9 4.5 %up.7.rest_0_ = bf16[512,1024]{1,0:T(8,128)(2,1)} custom-call(s32[1]{0:T(128)} %bitcast.15.z_ref, bf16[128,2048]{1,0:T(8,128)(2,1)S(1)} %collective-permute-done.24.rest_0_, bf16[128,2048]{1,0:T(8,128)(2,1)S(1)} %collective-permute-done.25.rest_1_, bf16[128,2048]{1,0:T(8,128)(2,1)S(1)} %collective-permute-done.26.rest_2_, ...), custom_call_target="tpu_custom_call" | custom-call | tf_op jit(solution)/shard_map/up/pallas_call | solution.py:376
  273.0 5.0 %down.4 = (bf16[768,1024]{1,0:T(8,128)(2,1)}, bf16[768,1024]{1,0:T(8,128)(2,1)}) custom-call(s32[1]{0:T(128)} %bitcast.15.z_ref, bf16[512,1024]{1,0:T(8,128)(2,1)S(1)} %up.4.rest_0_, bf16[512,1024]{1,0:T(8,128)(2,1)S(1)} %up.5.rest_1_, bf16[512,1024]{1,0:T(8,128)(2,1)S(1)} %up.6.rest_2_, bf16[1024,256]{1,0:T(8,128)(2,1)S(1)} %get-tuple-element.51.rest_3_.rest_1_, ...), custom_call_target="tpu_custom_call" | custom-call | tf_op jit(solution)/shard_map/down/pallas_call | solution.py:389
  281.8 10.8 %collective-permute-done.38 = bf16[256,1024]{1,0:T(8,128)(2,1)S(1)} collective-permute-done((bf16[256,1024]{1,0:T(8,128)(2,1)S(1)}, bf16[256,1024]{1,0:T(8,128)(2,1)S(1)}, u32[]{:S(2)}, u32[]{:S(2)}) %collective-permute-start.38) | collective-permute-done | bytes 524320 | tf_op jit(solution)/shard_map/ppermute | solution.py:214
  297.7 9.9 %collective-permute-done.39 = bf16[256,1024]{1,0:T(8,128)(2,1)S(1)} collective-permute-done((bf16[256,1024]{1,0:T(8,128)(2,1)S(1)}, bf16[256,1024]{1,0:T(8,128)(2,1)S(1)}, u32[]{:S(2)}, u32[]{:S(2)}) %collective-permute-start.39) | collective-permute-done | bytes 524320 | tf_op jit(solution)/shard_map/ppermute | solution.py:211
  308.5 8.9 %collective-permute-done.30 = bf16[256,1024]{1,0:T(8,128)(2,1)S(1)} collective-permute-done((bf16[256,1024]{1,0:T(8,128)(2,1)S(1)}, bf16[256,1024]{1,0:T(8,128)(2,1)S(1)}, u32[]{:S(2)}, u32[]{:S(2)}) %collective-permute-start.30) | collective-permute-done | bytes 524320 | tf_op jit(solution)/shard_map/ppermute | solution.py:214
  (154 shorter events, 45.7 us)
Async XLA Ops:
  69.3 28.3 %collective-permute-start.4 = (bf16[256,2048]{1,0:T(8,128)(2,1)}, bf16[256,2048]{1,0:T(8,128)(2,1)S(1)}, u32[]{:S(2)}, u32[]{:S(2)}) collective-permute-start(bf16[256,2048]{1,0:T(8,128)(2,1)} %get-tuple-element.48), channel_id=1, source_target_pairs={{0,1},{1,0},{2,3},{3,2},{4,5},{5,4},{6,7},{7,6},{8,9},{9,8},{10,11... | collective-permute-start | bytes 3145736 | tf_op jit(solution)/shard_map/ppermute | solution.py:211
  71.2 27.4 %collective-permute-start.6 = (bf16[256,2048]{1,0:T(8,128)(2,1)}, bf16[256,2048]{1,0:T(8,128)(2,1)S(1)}, u32[]{:S(2)}, u32[]{:S(2)}) collective-permute-start(bf16[256,2048]{1,0:T(8,128)(2,1)} %fusion), channel_id=1, source_target_pairs={{0,2},{1,3},{2,0},{3,1},{4,6},{5,7},{6,4},{7,5},{8,10},{9,11},{10,... | collective-permute-start | bytes 3145736 | tf_op jit(solution)/shard_map/ppermute | solution.py:211
  74.1 23.1 %collective-permute-start.9 = (bf16[256,1024]{1,0:T(8,128)(2,1)S(1)}, bf16[256,1024]{1,0:T(8,128)(2,1)S(1)}, u32[]{:S(2)}, u32[]{:S(2)}) collective-permute-start(bf16[256,1024]{1,0:T(8,128)(2,1)S(1)} %get-tuple-element.52), channel_id=1, source_target_pairs={{0,8},{4,12},{8,16},{12,20},{16,24},{20,28},{24,0},{28,4},{1,9},{5... | collective-permute-start | bytes 1572872 | tf_op jit(solution)/shard_map/ppermute | solution.py:214
  81.5 70.9 %collective-permute-start.11 = (bf16[256,1024]{1,0:T(8,128)(2,1)S(1)}, bf16[256,1024]{1,0:T(8,128)(2,1)S(1)}, u32[]{:S(2)}, u32[]{:S(2)}) collective-permute-start(bf16[256,1024]{1,0:T(8,128)(2,1)S(1)} %get-tuple-element.52), channel_id=1, source_target_pairs={{0,24},{4,28},{8,0},{12,4},{16,8},{20,12},{24,16},{28,20},{1,25},{... | collective-permute-start | bytes 1572872 | tf_op jit(solution)/shard_map/ppermute | solution.py:214
  84.4 68.0 %collective-permute-start.10 = (bf16[256,1024]{1,0:T(8,128)(2,1)S(1)}, bf16[256,1024]{1,0:T(8,128)(2,1)S(1)}, u32[]{:S(2)}, u32[]{:S(2)}) collective-permute-start(bf16[256,1024]{1,0:T(8,128)(2,1)S(1)} %get-tuple-element.53.rest_2_.rest_4_), channel_id=1, source_target_pairs={{0,16},{4,20},{8,24},{12,28},{16,0},{20,4},{24,8},{28,12},{1,17},{... | collective-permute-start | bytes 1572872 | tf_op jit(solution)/shard_map/ppermute | solution.py:214
  97.2 55.8 %collective-permute-start.12 = (bf16[256,1024]{1,0:T(8,128)(2,1)S(1)}, bf16[256,1024]{1,0:T(8,128)(2,1)S(1)}, u32[]{:S(2)}, u32[]{:S(2)}) collective-permute-start(bf16[256,1024]{1,0:T(8,128)(2,1)S(1)} %get-tuple-element.53.rest_2_.rest_4_), channel_id=1, source_target_pairs={{0,4},{4,0},{8,12},{12,8},{16,20},{20,16},{24,28},{28,24},{1,5},{5... | collective-permute-start | bytes 1572872 | tf_op jit(solution)/shard_map/ppermute | solution.py:214
  98.6 55.4 %collective-permute-start.19 = (bf16[1024,256]{1,0:T(8,128)(2,1)S(1)}, bf16[1024,256]{1,0:T(8,128)(2,1)S(1)}, u32[]{:S(2)}, u32[]{:S(2)}) collective-permute-start(bf16[1024,256]{1,0:T(8,128)(2,1)S(1)} %get-tuple-element.50), channel_id=1, source_target_pairs={{0,8},{4,12},{8,16},{12,20},{16,24},{20,28},{24,0},{28,4},{1,9},{5... | collective-permute-start | bytes 1572872 | tf_op jit(solution)/shard_map/ppermute | solution.py:214
  98.7 65.0 %collective-permute-start.20 = (bf16[1024,256]{1,0:T(8,128)(2,1)S(1)}, bf16[1024,256]{1,0:T(8,128)(2,1)S(1)}, u32[]{:S(2)}, u32[]{:S(2)}) collective-permute-start(bf16[1024,256]{1,0:T(8,128)(2,1)S(1)} %get-tuple-element.51.rest_3_.rest_1_), channel_id=1, source_target_pairs={{0,16},{4,20},{8,24},{12,28},{16,0},{20,4},{24,8},{28,12},{1,17},{... | collective-permute-start | bytes 1572872 | tf_op jit(solution)/shard_map/ppermute | solution.py:214
  152.4 46.9 %collective-permute-start.16 = (bf16[256,2048]{1,0:T(8,128)(2,1)S(1)}, bf16[256,2048]{1,0:T(8,128)(2,1)S(1)}, u32[]{:S(2)}, u32[]{:S(2)}) collective-permute-start(bf16[256,2048]{1,0:T(8,128)(2,1)S(1)} %get-tuple-element.26.rest_0_), channel_id=1, source_target_pairs={{0,8},{4,12},{8,0},{12,4},{16,24},{20,28},{24,16},{28,20},{1,9},{5... | collective-permute-start | bytes 3145736 | tf_op jit(solution)/shard_map/ppermute | solution.py:214
  152.4 46.9 %collective-permute-start.7 = (bf16[256,2048]{1,0:T(8,128)(2,1)S(1)}, bf16[256,2048]{1,0:T(8,128)(2,1)S(1)}, u32[]{:S(2)}, u32[]{:S(2)}) collective-permute-start(bf16[256,2048]{1,0:T(8,128)(2,1)S(1)} %get-tuple-element.26.rest_0_), channel_id=1, source_target_pairs={{0,2},{1,3},{2,0},{3,1},{4,6},{5,7},{6,4},{7,5},{8,10},{9,11},{10,... | collective-permute-start | bytes 3145736 | tf_op jit(solution)/shard_map/ppermute | solution.py:211
  153.0 44.3 %collective-permute-start.21 = (bf16[1024,256]{1,0:T(8,128)(2,1)S(1)}, bf16[1024,256]{1,0:T(8,128)(2,1)S(1)}, u32[]{:S(2)}, u32[]{:S(2)}) collective-permute-start(bf16[1024,256]{1,0:T(8,128)(2,1)S(1)} %get-tuple-element.50), channel_id=1, source_target_pairs={{0,24},{4,28},{8,0},{12,4},{16,8},{20,12},{24,16},{28,20},{1,25},{... | collective-permute-start | bytes 1572872 | tf_op jit(solution)/shard_map/ppermute | solution.py:214
  154.0 43.3 %collective-permute-start.31 = (bf16[1024,256]{1,0:T(8,128)(2,1)S(1)}, bf16[1024,256]{1,0:T(8,128)(2,1)S(1)}, u32[]{:S(2)}, u32[]{:S(2)}) collective-permute-start(bf16[1024,256]{1,0:T(8,128)(2,1)S(1)} %get-tuple-element.51.rest_3_.rest_1_), channel_id=1, source_target_pairs={{0,4},{4,0},{8,12},{12,8},{16,20},{20,16},{24,28},{28,24},{1,5},{5... | collective-permute-start | bytes 1572872 | tf_op jit(solution)/shard_map/ppermute | solution.py:214
  163.7 34.1 %collective-permute-start.13 = (bf16[256,1024]{1,0:T(8,128)(2,1)S(1)}, bf16[256,1024]{1,0:T(8,128)(2,1)S(1)}, u32[]{:S(2)}, u32[]{:S(2)}) collective-permute-start(bf16[256,1024]{1,0:T(8,128)(2,1)S(1)} %collective-permute-done.9.rest_3_.rest_5_), channel_id=1, source_target_pairs={{0,4},{4,0},{8,12},{12,8},{16,20},{20,16},{24,28},{28,24},{1,5},{5... | collective-permute-start | bytes 1572872 | tf_op jit(solution)/shard_map/ppermute | solution.py:214
  197.3 25.6 %collective-permute-start.18 = (bf16[256,2048]{1,0:T(8,128)(2,1)S(1)}, bf16[256,2048]{1,0:T(8,128)(2,1)S(1)}, u32[]{:S(2)}, u32[]{:S(2)}) collective-permute-start(bf16[256,2048]{1,0:T(8,128)(2,1)S(1)} %get-tuple-element.26.rest_0_), channel_id=1, source_target_pairs={{0,1},{1,0},{2,3},{3,2},{4,5},{5,4},{6,7},{7,6},{8,9},{9,8},{10,11... | collective-permute-start | bytes 3145736 | tf_op jit(solution)/shard_map/ppermute | solution.py:211
  197.3 14.8 %collective-permute-start.14 = (bf16[256,1024]{1,0:T(8,128)(2,1)S(1)}, bf16[256,1024]{1,0:T(8,128)(2,1)S(1)}, u32[]{:S(2)}, u32[]{:S(2)}) collective-permute-start(bf16[256,1024]{1,0:T(8,128)(2,1)S(1)} %collective-permute-done.10.rest_4_.rest_6_), channel_id=1, source_target_pairs={{0,4},{4,0},{8,12},{12,8},{16,20},{20,16},{24,28},{28,24},{1,5},{5... | collective-permute-start | bytes 1572872 | tf_op jit(solution)/shard_map/ppermute | solution.py:214
  197.8 25.0 %collective-permute-start.15 = (bf16[256,1024]{1,0:T(8,128)(2,1)S(1)}, bf16[256,1024]{1,0:T(8,128)(2,1)S(1)}, u32[]{:S(2)}, u32[]{:S(2)}) collective-permute-start(bf16[256,1024]{1,0:T(8,128)(2,1)S(1)} %collective-permute-done.11.rest_5_.rest_7_), channel_id=1, source_target_pairs={{0,4},{4,0},{8,12},{12,8},{16,20},{20,16},{24,28},{28,24},{1,5},{5... | collective-permute-start | bytes 1572872 | tf_op jit(solution)/shard_map/ppermute | solution.py:214
  199.3 37.5 %collective-permute-start.17 = (bf16[256,2048]{1,0:T(8,128)(2,1)S(1)}, bf16[256,2048]{1,0:T(8,128)(2,1)S(1)}, u32[]{:S(2)}, u32[]{:S(2)}) collective-permute-start(bf16[256,2048]{1,0:T(8,128)(2,1)S(1)} %collective-permute-done.16.rest_0_), channel_id=1, source_target_pairs={{0,1},{1,0},{2,3},{3,2},{4,5},{5,4},{6,7},{7,6},{8,9},{9,8},{10,11... | collective-permute-start | bytes 3145736 | tf_op jit(solution)/shard_map/ppermute | solution.py:211
  199.4 37.5 %collective-permute-start.8 = (bf16[256,2048]{1,0:T(8,128)(2,1)S(1)}, bf16[256,2048]{1,0:T(8,128)(2,1)S(1)}, u32[]{:S(2)}, u32[]{:S(2)}) collective-permute-start(bf16[256,2048]{1,0:T(8,128)(2,1)S(1)} %collective-permute-done.7.rest_0_), channel_id=1, source_target_pairs={{0,1},{1,0},{2,3},{3,2},{4,5},{5,4},{6,7},{7,6},{8,9},{9,8},{10,11... | collective-permute-start | bytes 3145736 | tf_op jit(solution)/shard_map/ppermute | solution.py:211
  222.9 13.5 %collective-permute-start.25 = (bf16[128,2048]{1,0:T(8,128)(2,1)S(1)}, bf16[128,2048]{1,0:T(8,128)(2,1)S(1)}, u32[]{:S(2)}, u32[]{:S(2)}) collective-permute-start(bf16[128,2048]{1,0:T(8,128)(2,1)S(1)} %slice.134), channel_id=1, source_target_pairs={{0,8},{4,12},{8,0},{12,4},{16,24},{20,28},{24,16},{28,20},{1,9},{5... | collective-permute-start | bytes 1572872 | tf_op jit(solution)/shard_map/ppermute | solution.py:214
  222.9 27.2 %collective-permute-start.32 = (bf16[1024,256]{1,0:T(8,128)(2,1)S(1)}, bf16[1024,256]{1,0:T(8,128)(2,1)S(1)}, u32[]{:S(2)}, u32[]{:S(2)}) collective-permute-start(bf16[1024,256]{1,0:T(8,128)(2,1)S(1)} %collective-permute-done.19.rest_4_.rest_2_), channel_id=1, source_target_pairs={{0,4},{4,0},{8,12},{12,8},{16,20},{20,16},{24,28},{28,24},{1,5},{5... | collective-permute-start | bytes 1572872 | tf_op jit(solution)/shard_map/ppermute | solution.py:214
  225.1 25.0 %collective-permute-start.33 = (bf16[1024,256]{1,0:T(8,128)(2,1)S(1)}, bf16[1024,256]{1,0:T(8,128)(2,1)S(1)}, u32[]{:S(2)}, u32[]{:S(2)}) collective-permute-start(bf16[1024,256]{1,0:T(8,128)(2,1)S(1)} %collective-permute-done.20.rest_5_.rest_3_), channel_id=1, source_target_pairs={{0,4},{4,0},{8,12},{12,8},{16,20},{20,16},{24,28},{28,24},{1,5},{5... | collective-permute-start | bytes 1572872 | tf_op jit(solution)/shard_map/ppermute | solution.py:214
  236.3 22.6 %collective-permute-start.34 = (bf16[1024,256]{1,0:T(8,128)(2,1)S(1)}, bf16[1024,256]{1,0:T(8,128)(2,1)S(1)}, u32[]{:S(2)}, u32[]{:S(2)}) collective-permute-start(bf16[1024,256]{1,0:T(8,128)(2,1)S(1)} %collective-permute-done.21.rest_6_.rest_4_), channel_id=1, source_target_pairs={{0,4},{4,0},{8,12},{12,8},{16,20},{20,16},{24,28},{28,24},{1,5},{5... | collective-permute-start | bytes 1572872 | tf_op jit(solution)/shard_map/ppermute | solution.py:214
  236.9 27.0 %collective-permute-start.26 = (bf16[128,2048]{1,0:T(8,128)(2,1)S(1)}, bf16[128,2048]{1,0:T(8,128)(2,1)S(1)}, u32[]{:S(2)}, u32[]{:S(2)}) collective-permute-start(bf16[128,2048]{1,0:T(8,128)(2,1)S(1)} %collective-permute-done.24.rest_0_), channel_id=1, source_target_pairs={{0,1},{1,0},{2,3},{3,2},{4,5},{5,4},{6,7},{7,6},{8,9},{9,8},{10,11... | collective-permute-start | bytes 1572872 | tf_op jit(solution)/shard_map/ppermute | solution.py:211
  236.9 27.0 %collective-permute-start.27 = (bf16[128,2048]{1,0:T(8,128)(2,1)S(1)}, bf16[128,2048]{1,0:T(8,128)(2,1)S(1)}, u32[]{:S(2)}, u32[]{:S(2)}) collective-permute-start(bf16[128,2048]{1,0:T(8,128)(2,1)S(1)} %collective-permute-done.25.rest_1_), channel_id=1, source_target_pairs={{0,1},{1,0},{2,3},{3,2},{4,5},{5,4},{6,7},{7,6},{8,9},{9,8},{10,11... | collective-permute-start | bytes 1572872 | tf_op jit(solution)/shard_map/ppermute | solution.py:211
  263.9 17.4 %collective-permute-start.35 = (bf16[768,1024]{1,0:T(8,128)(2,1)}, bf16[768,1024]{1,0:T(8,128)(2,1)S(1)}, u32[]{:S(2)}, u32[]{:S(2)}) collective-permute-start(bf16[768,1024]{1,0:T(8,128)(2,1)} %get-tuple-element.35), channel_id=1, source_target_pairs={{0,1},{1,0},{2,3},{3,2},{4,5},{5,4},{6,7},{7,6},{8,9},{9,8},{10,11... | collective-permute-start | bytes 4718600 | tf_op jit(solution)/shard_map/ppermute | solution.py:211
  278.0 17.1 %collective-permute-start.22 = (bf16[768,1024]{1,0:T(8,128)(2,1)}, bf16[768,1024]{1,0:T(8,128)(2,1)S(1)}, u32[]{:S(2)}, u32[]{:S(2)}) collective-permute-start(bf16[768,1024]{1,0:T(8,128)(2,1)} %get-tuple-element.28), channel_id=1, source_target_pairs={{0,1},{1,0},{2,3},{3,2},{4,5},{5,4},{6,7},{7,6},{8,9},{9,8},{10,11... | collective-permute-start | bytes 4718600 | tf_op jit(solution)/shard_map/ppermute | solution.py:211
  278.7 13.9 %collective-permute-start.38 = (bf16[256,1024]{1,0:T(8,128)(2,1)S(1)}, bf16[256,1024]{1,0:T(8,128)(2,1)S(1)}, u32[]{:S(2)}, u32[]{:S(2)}) collective-permute-start(bf16[256,1024]{1,0:T(8,128)(2,1)S(1)} %convert_add_fusion.1), channel_id=1, source_target_pairs={{0,8},{4,12},{8,0},{12,4},{16,24},{20,28},{24,16},{28,20},{1,9},{5... | collective-permute-start | bytes 1572872 | tf_op jit(solution)/shard_map/ppermute | solution.py:214
  280.6 15.0 %collective-permute-start.29 = (bf16[256,1024]{1,0:T(8,128)(2,1)S(1)}, bf16[256,1024]{1,0:T(8,128)(2,1)S(1)}, u32[]{:S(2)}, u32[]{:S(2)}) collective-permute-start(bf16[256,1024]{1,0:T(8,128)(2,1)S(1)} %convert_add_fusion.6), channel_id=1, source_target_pairs={{0,2},{1,3},{2,0},{3,1},{4,6},{5,7},{6,4},{7,5},{8,10},{9,11},{10,... | collective-permute-start | bytes 1572872 | tf_op jit(solution)/shard_map/ppermute | solution.py:211
  292.8 14.9 %collective-permute-start.39 = (bf16[256,1024]{1,0:T(8,128)(2,1)S(1)}, bf16[256,1024]{1,0:T(8,128)(2,1)S(1)}, u32[]{:S(2)}, u32[]{:S(2)}) collective-permute-start(bf16[256,1024]{1,0:T(8,128)(2,1)S(1)} %add_convert_fusion.1), channel_id=1, source_target_pairs={{0,2},{1,3},{2,0},{3,1},{4,6},{5,7},{6,4},{7,5},{8,10},{9,11},{10,... | collective-permute-start | bytes 1572872 | tf_op jit(solution)/shard_map/ppermute | solution.py:211
  293.4 14.8 %collective-permute-start.36 = (bf16[256,1024]{1,0:T(8,128)(2,1)S(1)}, bf16[256,1024]{1,0:T(8,128)(2,1)S(1)}, u32[]{:S(2)}, u32[]{:S(2)}) collective-permute-start(bf16[256,1024]{1,0:T(8,128)(2,1)S(1)} %convert_add_fusion.3), channel_id=1, source_target_pairs={{0,8},{4,12},{8,0},{12,4},{16,24},{20,28},{24,16},{28,20},{1,9},{5... | collective-permute-start | bytes 1572872 | tf_op jit(solution)/shard_map/ppermute | solution.py:214
  295.9 21.5 %collective-permute-start.30 = (bf16[256,1024]{1,0:T(8,128)(2,1)S(1)}, bf16[256,1024]{1,0:T(8,128)(2,1)S(1)}, u32[]{:S(2)}, u32[]{:S(2)}) collective-permute-start(bf16[256,1024]{1,0:T(8,128)(2,1)S(1)} %add_convert_fusion.2), channel_id=1, source_target_pairs={{0,8},{4,12},{8,0},{12,4},{16,24},{20,28},{24,16},{28,20},{1,9},{5... | collective-permute-start | bytes 1572872 | tf_op jit(solution)/shard_map/ppermute | solution.py:214
  296.3 21.1 %collective-permute-start.23 = (bf16[256,1024]{1,0:T(8,128)(2,1)S(1)}, bf16[256,1024]{1,0:T(8,128)(2,1)S(1)}, u32[]{:S(2)}, u32[]{:S(2)}) collective-permute-start(bf16[256,1024]{1,0:T(8,128)(2,1)S(1)} %convert_add_fusion.9), channel_id=1, source_target_pairs={{0,2},{1,3},{2,0},{3,1},{4,6},{5,7},{6,4},{7,5},{8,10},{9,11},{10,... | collective-permute-start | bytes 1572872 | tf_op jit(solution)/shard_map/ppermute | solution.py:211
  (33 other events, 497.2 us)

commit v2 on v1

--- a/solution.py
+++ b/solution.py
@@ -54,7 +54,21 @@
     return first * cosine - second * sine, first * sine + second * cosine
 
 
-def state_kernel(key_ref, value_ref, decay_ref, table_ref, out_ref, kd_ref, *, halves):
+def with_decay(out_ref, state, decay):
+    size = state.shape[0]
+    high = decay.astype(BF).astype(F32)
+    row = lax.broadcasted_iota(jnp.int32, (TAIL, DV), 0)
+    out_ref[:size, :] = state.astype(BF)
+    out_ref[size:, :] = jnp.where(row == 0, high, decay - high).astype(BF)
+
+
+def parts_of(payload):
+    size = payload.shape[0] - TAIL
+    wide = payload.astype(F32)
+    return wide[size : size + 1, :] + wide[size + 1 : size + 2, :], wide[:size, :]
+
+
+def state_kernel(y_ref, key_ref, value_ref, decay_ref, table_ref, mine_ref, theirs_ref, kd_ref, *, halves):
     blocks = decay_ref.shape[1]
     _, col, _, before, whole = decay_sums(decay_ref[0])
     scale = DK ** (-0.5)
@@ -65,15 +79,59 @@
         factor = jnp.exp(whole - before[n : n + 1, :] - jnp.broadcast_to(col[:, n : n + 1], (BLOCK, BLOCK)))
         kd_ref[rows, : DK // 2] = (a * factor).astype(BF)
         kd_ref[rows, DK // 2 :] = (b * factor).astype(BF)
-    state = dot(kd_ref[...], value_ref[...], ((0,), (0,))).astype(BF)
-    decay = jnp.broadcast_to(jnp.exp(whole[:, :1]), (TAIL, DV))
-    high = decay.astype(BF).astype(F32)
-    row = lax.broadcasted_iota(jnp.int32, (TAIL, DV), 0)
-    tail = jnp.where(row == 0, high, decay - high).astype(BF)
+    state = dot(kd_ref[...], value_ref[...], ((0,), (0,)))
+    decay = jnp.broadcast_to(jnp.exp(whole[:, :1]), (1, DV))
     size = DK // halves
     for j in range(halves):
-        out_ref[j, :size, :] = state[j * size : (j + 1) * size, :]
-        out_ref[j, size:, :] = tail
+        half = pl.program_id(0) * halves + j
+
+        @pl.when(half == y_ref[0])
+        def _():
+            with_decay(mine_ref, state[j * size : (j + 1) * size, :], decay)
+
+        @pl.when(half != y_ref[0])
+        def _():
+            with_decay(theirs_ref, state[j * size : (j + 1) * size, :], decay)
+
+
+def in_order(y_ref, mine_ref, got_ref):
+    (mine_decay, mine), (got_decay, got) = parts_of(mine_ref[...]), parts_of(got_ref[...])
+    lower = y_ref[0] == 0
+    return (
+        (jnp.where(lower, mine_decay, got_decay), jnp.where(lower, mine, got)),
+        (jnp.where(lower, got_decay, mine_decay), jnp.where(lower, got, mine)),
+    )
+
+
+def before_of(sent):
+    decay, before = parts_of(sent[0][...])
+    for ref in sent[1:]:
+        far_decay, far_state = parts_of(ref[...])
+        before = decay * far_state + before
+        decay = decay * far_decay
+    return decay, before
+
+
+def plane_kernel(y_ref, mine_ref, got_ref, out_ref):
+    (first_decay, first), (second_decay, second) = in_order(y_ref, mine_ref, got_ref)
+    with_decay(out_ref, second_decay * first + second, second_decay * first_decay)
+
+
+def upto_kernel(plane_ref, *rest):
+    sent, out_ref = rest[:-1], rest[-1]
+    decay, before = before_of(sent)
+    plane_decay, plane = parts_of(plane_ref[...])
+    with_decay(out_ref, plane_decay * before + plane, plane_decay * decay)
+
+
+def before_kernel(y_ref, mine_ref, got_ref, *rest):
+    sent, (send_ref, keep_ref) = rest[:-2], rest[-2:]
+    (first_decay, first), _ = in_order(y_ref, mine_ref, got_ref)
+    before = before_of(sent)[1]
+    after = first_decay * before + first
+    lower = y_ref[0] == 0
+    send_ref[...] = jnp.where(lower, after, before).astype(BF)
+    keep_ref[...] = jnp.where(lower, before, after).astype(BF)
 
 
 def local_kernel(query_ref, key_ref, value_ref, decay_ref, table_ref, out_ref, qd_ref, state_ref):
@@ -119,11 +177,20 @@
                 state_ref[...] = term
 
 
-def gate_kernel(order_ref, local_ref, qd_ref, in_ref, gate_ref, weight_ref, out_ref, gated_ref):
+def gate_kernel(order_ref, y_ref, local_ref, qd_ref, keep_ref, sent_ref, gate_ref, weight_ref, out_ref, gated_ref, in_ref):
     heads = local_ref.shape[1] // DV
+    size = keep_ref.shape[0]
+
+    @pl.when(pl.program_id(0) == 0)
+    def _():
+        in_ref[y_ref[0]] = keep_ref[...]
+        in_ref[1 - y_ref[0]] = sent_ref[...]
+
     for h in range(heads):
         cols = pl.ds(h * DV, DV)
-        retained = local_ref[:, cols] + dot(qd_ref[:, pl.ds(h * DK, DK)], in_ref[h])
+        retained = local_ref[:, cols]
+        for j in range(h * DK // size, (h + 1) * DK // size):
+            retained = retained + dot(qd_ref[:, pl.ds(j * size, size)], in_ref[j])
         mean = jnp.mean(retained * retained, axis=-1, keepdims=True)
         gate = gate_ref[:, cols].astype(F32)
         silu = gate / (1.0 + jnp.exp(-gate))
@@ -262,16 +329,20 @@
         decay_spec = pl.BlockSpec((1, blocks, BLOCK), lambda h: (h, 0, 0))
         key_spec = pl.BlockSpec((rows, DK), lambda h: (0, h))
         value_spec = pl.BlockSpec((rows, DV), lambda h: (0, h))
-        own_state = pl.pallas_call(
+        y_word = y.astype(jnp.int32).reshape(1)
+        payload = jax.ShapeDtypeStruct((size + TAIL, DV), BF)
+        payload_spec = pl.BlockSpec(payload.shape, lambda h: (0, 0))
+        word_spec = pl.BlockSpec(memory_space=pltpu.SMEM)
+        mine, theirs = pl.pallas_call(
             functools.partial(state_kernel, halves=halves),
-            out_shape=jax.ShapeDtypeStruct((2, size + TAIL, DV), BF),
+            out_shape=(payload, payload),
             grid=(heads,),
-            in_specs=[key_spec, value_spec, decay_spec, table_spec],
-            out_specs=pl.BlockSpec((halves, size + TAIL, DV), lambda h: (h, 0, 0)),
+            in_specs=[word_spec, key_spec, value_spec, decay_spec, table_spec],
+            out_specs=(payload_spec, payload_spec),
             scratch_shapes=[pltpu.VMEM((rows, DK), BF)],
             compiler_params=params(),
             name="state",
-        )(keys, values, decay, table)
+        )(y_word, keys, values, decay, table)
 
         local, query_decayed = pl.pallas_call(
             local_kernel,
@@ -287,39 +358,25 @@
             name="local",
         )(queries, keys, values, decay, table)
 
-        def parts(payload):
-            wide = payload.astype(F32)
-            return wide[size, 0] + wide[size + 1, 0], wide[:size]
-
-        def pick(pair, index):
-            return lax.dynamic_index_in_dim(pair, index, 0, keepdims=False)
-
-        got = swap_y(pick(own_state, 1 - y))
-        mine = pick(own_state, y)
-        first = jnp.where(y == 0, mine, got)
-        second = jnp.where(y == 0, got, mine)
-        (first_decay, first_state), (second_decay, second_state) = parts(first), parts(second)
-        plane_decay = first_decay * second_decay
-        plane_state = second_decay * first_state + second_state
-        row = lax.broadcasted_iota(jnp.int32, (TAIL, DV), 0)
-        before_decay, before = jnp.ones((), F32), jnp.zeros((size, DV), F32)
-        reach = 1
+        def small(kernel, out_shape, *args):
+            return pl.pallas_call(
+                kernel,
+                out_shape=out_shape,
+                in_specs=[word_spec if arg is y_word else pl.BlockSpec(memory_space=pltpu.VMEM) for arg in args],
+                compiler_params=params(),
+            )(*args)
+
+        got = swap_y(theirs)
+        plane = upto = small(plane_kernel, payload, y_word, mine, got)
+        sent = [forward_z(plane, 1)]
+        reach = 2
         while reach < n_z:
-            upto_decay = before_decay * plane_decay
-            upto = plane_decay * before + plane_state
-            high = upto_decay.astype(BF).astype(F32)
-            tail = jnp.where(row == 0, high, upto_decay - high)
-            sent = forward_z(jnp.concatenate([upto, tail], axis=0).astype(BF), reach)
-            far_decay, far_state = parts(sent)
-            before = before_decay * far_state + before
-            before_decay = before_decay * far_decay
+            upto = small(upto_kernel, payload, plane, *sent)
+            sent.append(forward_z(upto, reach))
             reach *= 2
-        after_first = (first_decay * before + first_state).astype(BF)
-        before = before.astype(BF)
-        sent = swap_y(jnp.where(y == 0, after_first, before))
-        kept = jnp.where(y == 0, before, after_first)
-        incoming = jnp.stack([jnp.where(y == 0, kept, sent), jnp.where(y == 0, sent, kept)])
-        incoming = incoming.reshape(heads, DK, DV)
+        state_half = jax.ShapeDtypeStruct((size, DV), BF)
+        send, keep = small(before_kernel, (state_half, state_half), y_word, mine, got, *sent)
+        arrived_state = swap_y(send)
 
         def projected(order):
             count = order.shape[0]
@@ -327,20 +384,21 @@
                 gate_kernel,
                 out_shape=jax.ShapeDtypeStruct((count, own_rows, width), BF),
                 grid_spec=pltpu.PrefetchScalarGridSpec(
-                    num_scalar_prefetch=1,
+                    num_scalar_prefetch=2,
                     grid=(count,),
                     in_specs=[
-                        pl.BlockSpec((own_rows, heads * DV), lambda j, o: (o[j], 0)),
-                        pl.BlockSpec((own_rows, heads * DK), lambda j, o: (o[j], 0)),
-                        pl.BlockSpec((heads, DK, DV), lambda j, o: (0, 0, 0)),
-                        pl.BlockSpec((own_rows, heads * DV), lambda j, o: (o[j], 0)),
-                        pl.BlockSpec(out_weight.shape, lambda j, o: (0, 0)),
+                        pl.BlockSpec((own_rows, heads * DV), lambda j, o, w: (o[j], 0)),
+                        pl.BlockSpec((own_rows, heads * DK), lambda j, o, w: (o[j], 0)),
+                        pl.BlockSpec((size, DV), lambda j, o, w: (0, 0)),
+                        pl.BlockSpec((size, DV), lambda j, o, w: (0, 0)),
+                        pl.BlockSpec((own_rows, heads * DV), lambda j, o, w: (o[j], 0)),
+                        pl.BlockSpec(out_weight.shape, lambda j, o, w: (0, 0)),
                     ],
-                    out_specs=pl.BlockSpec((1, own_rows, width), lambda j, o: (j, 0, 0)),
-                    scratch_shapes=[pltpu.VMEM((own_rows, heads * DV), BF)],
+                    out_specs=pl.BlockSpec((1, own_rows, width), lambda j, o, w: (j, 0, 0)),
+                    scratch_shapes=[pltpu.VMEM((own_rows, heads * DV), BF), pltpu.VMEM((2, size, DV), BF)],
                 ),
                 compiler_params=params(),
-            )(order, local, query_decayed, incoming, gates, out_weight)
+            )(order, y_word, local, query_decayed, keep, arrived_state, gates, out_weight)
 
         def places_of(steps):
             chips = [2 * ((x + s) % n_x) for s in steps]
@@ -355,7 +413,6 @@
         steps = max(own_rows // 128, 1)
         tall = own_rows // steps
         row_spec = pl.BlockSpec((tall, width), lambda i, o: (i, 0))
-        y_word = y.astype(jnp.int32).reshape(1)
         updated, normed = pl.pallas_call(
             functools.partial(norm_kernel, regions=n_sp),
             out_shape=(jax.ShapeDtypeStruct(resid.shape, BF), jax.ShapeDtypeStruct(resid.shape, BF)),
@@ -402,13 +459,15 @@
 
         near_x = range(1, n_x)
         top = own_rows // 2
-        from_x = {s: shift_x(normed, s) for s in near_x}
-        from_z = swap_z(normed)
-        corner = {s: [shift_x(from_z[:top], s), swap_z(from_x[s][top:])] for s in near_x}
-        chunks = {"o": [normed], "z": [from_z]}
+        upper, under = normed[:top], normed[top:]
+        x_under = {s: shift_x(under, s) for s in near_x}
+        z_upper = swap_z(upper)
+        x_upper = {s: shift_x(upper, s) for s in near_x}
+        z_under = swap_z(under)
+        chunks = {"o": [normed], "z": [z_upper, z_under]}
         for s in near_x:
-            chunks[f"x{s}"] = [from_x[s]]
-            chunks[f"c{s}"] = corner[s]
+            chunks[f"x{s}"] = [x_upper[s], x_under[s]]
+            chunks[f"c{s}"] = [shift_x(z_upper, s), swap_z(x_under[s])]
         hidden = {key: raised(parts + [swap_core(part) for part in parts]) for key, parts in chunks.items()}
         straight = [hidden[f"x{s}"] for s in near_x] + [hidden["z"], hidden["o"]]
         corners = [hidden[f"c{s}"] for s in near_x]
@@ -416,9 +475,11 @@
         def home(value, s):
             return shift_x(value.astype(BF), n_x - s).astype(F32)
 
-        *left_x, left_z, left_sum = lowered(straight, 0)
+        (left_z,) = lowered([hidden["z"]], 0)
+        *left_x, left_sum = lowered(straight[:-2] + straight[-1:], 0)
         left_c = lowered(corners, 0)
-        *right_x, right_z, right_sum = lowered(straight, 1)
+        (right_z,) = lowered([hidden["z"]], 1)
+        *right_x, right_sum = lowered(straight[:-2] + straight[-1:], 1)
         right_c = lowered(corners, 1)
         for s in near_x:
             left_sum = left_sum + home(left_x[s - 1], s)

time: 319 us -> 303 us (0.950)
  waiting for transfers between devices: 181 us -> 139 us
  starting transfers between devices: 56.6 us -> 75.8 us
  Pallas kernels: 55.7 us -> 61.2 us
  local copies, waits for them, and re-layouts: 13.5 us -> 18.1 us
  between operations: 4.31 us -> 0.42 us
    ppermute x23 -> x24, waiting for transfers between devices: 169 us -> 120 us  [over_sp(): return lax.ppermute(value, 'sp', pairs)]
    ppermute x23 -> x24, starting transfers between devices: 48.6 us -> 64.8 us  [over_sp(): return lax.ppermute(value, 'sp', pairs)]
    ppermute x17 -> x22, waiting for transfers between devices: 11.6 us -> 18.7 us  [over_tp(): return lax.ppermute(value, 'tp', [(t, turn(t)) for t in range(n_tp)])]
    unnamed x51 -> x47, local copies, waits for them, and re-layouts: 9.48 us -> 15.4 us
    add x6 -> x7, other arithmetic: 1.48 us -> 5.59 us  [lowered(): sums = [mine[part].astype(F32) + others[part].astype(F32) for part in parts]]
    ppermute x17 -> x22, starting transfers between devices: 8.02 us -> 10.9 us  [over_tp(): return lax.ppermute(value, 'tp', [(t, turn(t)) for t in range(n_tp)])]
    pallas_call x4 -> x6, Pallas kernels: 12.8 us -> 14.9 us  [lowered(): pl.pallas_call(functools.partial(down_kernel, planes=n_z), out_shape=(jax...]
  transfers between devices with their start and end apart: 40 -> 46, of which waited for: 16 -> 18; matrix products, arithmetic and copies ran while one was open for 2% -> 3% of each run, Pallas kernels for 14% -> 16%
where the time goes in v2:
time: 303 us
  waiting for transfers between devices  139 us (46%)
  starting transfers between devices  75.8 us (25%)
  Pallas kernels  61.2 us (20%)
  local copies, waits for them, and re-layouts  18.1 us (6%)
  other arithmetic  8.41 us (3%)
    ppermute x24, waiting for transfers between devices, over_sp(): return lax.ppermute(value, 'sp', pairs)  120 us
    ppermute x24, starting transfers between devices, over_sp(): return lax.ppermute(value, 'sp', pairs)  64.8 us
    ppermute x22, waiting for transfers between devices, over_tp(): return lax.ppermute(value, 'tp', [(t, turn(t)) for t in range(n_tp)])  18.7 us
    pallas_call x4, Pallas kernels, raised(): pl.pallas_call(functools.partial(up_kernel, planes=n_z, sources=len(sourc...  17.9 us
    unnamed x47, local copies, waits for them, and re-layouts  15.4 us
    pallas_call x6, Pallas kernels, lowered(): pl.pallas_call(functools.partial(down_kernel, planes=n_z), out_shape=(jax...  14.9 us
    pallas_call x2, Pallas kernels, projected(): pl.pallas_call(gate_kernel, out_shape=jax.ShapeDtypeStruct((count, own_ro...  13.1 us
    ppermute x22, starting transfers between devices, over_tp(): return lax.ppermute(value, 'tp', [(t, turn(t)) for t in range(n_tp)])  10.9 us
  transfers between devices with their start and end apart: 46, of which 18 were waited for; matrix products, arithmetic and copies ran while one was open for 3% of the time, Pallas kernels for 16%

profile of v2, /device:TPU:0, one launch (start us, length us, event | category | flops | bytes accessed | tf_op | source)
XLA Modules:
  0.0 302.5 jit_solution(8390482472034930642)
XLA Ops:
  3.9 3.2 %state.1 = (bf16[272,512]{1,0:T(8,128)(2,1)S(1)}, bf16[272,512]{1,0:T(8,128)(2,1)S(1)}) custom-call(s32[1]{0:T(128)} %bitcast.y_ref, bf16[1024,512]{1,0:T(8,128)(2,1)S(1)} %copy-done.12, bf16[1024,1024]{1,0:T(8,128)(2,1)S(1)} %copy-done.8, f32[2,8,128]{2,1,0:T(8,128)S(1)} %bitcast.16, f32[2,136,128]{2,1,0:T(8,128)S(1)} %pad_maximum_fusion.table_ref), custom_call_target="tpu_custom_call" | custom-call | tf_op jit(solution)/shard_map/state/pallas_call | solution.py:336
  10.2 6.6 %collective-permute-done.got_ref = bf16[272,512]{1,0:T(8,128)(2,1)S(1)} collective-permute-done((bf16[272,512]{1,0:T(8,128)(2,1)S(1)}, bf16[272,512]{1,0:T(8,128)(2,1)S(1)}, u32[]{:S(2)}, u32[]{:S(2)}) %collective-permute-start) | collective-permute-done | bytes 278560 | tf_op jit(solution)/shard_map/ppermute | solution.py:281
  17.0 3.7 %collective-permute-start.1 = (bf16[272,512]{1,0:T(8,128)(2,1)S(1)}, bf16[272,512]{1,0:T(8,128)(2,1)S(1)}, u32[]{:S(2)}, u32[]{:S(2)}) collective-permute-start(bf16[272,512]{1,0:T(8,128)(2,1)S(1)} %shard_map.100.plane_ref), channel_id=1, source_target_pairs={{0,8},{4,12},{8,16},{12,20},{16,24},{20,28},{1,9},{5,13},{9,17},{1... | collective-permute-start | bytes 835592 | tf_op jit(solution)/shard_map/ppermute | solution.py:281
  20.7 5.0 %collective-permute-done.1.rest_0_ = bf16[272,512]{1,0:T(8,128)(2,1)S(1)} collective-permute-done((bf16[272,512]{1,0:T(8,128)(2,1)S(1)}, bf16[272,512]{1,0:T(8,128)(2,1)S(1)}, u32[]{:S(2)}, u32[]{:S(2)}) %collective-permute-start.1) | collective-permute-done | bytes 278560 | tf_op jit(solution)/shard_map/ppermute | solution.py:281
  25.8 5.4 %collective-permute-start.2 = (bf16[272,512]{1,0:T(8,128)(2,1)S(1)}, bf16[272,512]{1,0:T(8,128)(2,1)S(1)}, u32[]{:S(2)}, u32[]{:S(2)}) collective-permute-start(bf16[272,512]{1,0:T(8,128)(2,1)S(1)} %shard_map.101), channel_id=1, source_target_pairs={{0,16},{4,20},{8,24},{12,28},{1,17},{5,21},{9,25},{13,29},{2,18},{... | collective-permute-start | bytes 835592 | tf_op jit(solution)/shard_map/ppermute | solution.py:281
  31.3 4.2 %collective-permute-done.2.rest_1_ = bf16[272,512]{1,0:T(8,128)(2,1)S(1)} collective-permute-done((bf16[272,512]{1,0:T(8,128)(2,1)S(1)}, bf16[272,512]{1,0:T(8,128)(2,1)S(1)}, u32[]{:S(2)}, u32[]{:S(2)}) %collective-permute-start.2) | collective-permute-done | bytes 278560 | tf_op jit(solution)/shard_map/ppermute | solution.py:281
  41.9 7.6 %local.1 = (f32[1024,1024]{1,0:T(8,128)}, bf16[1024,512]{1,0:T(8,128)(2,1)S(1)}) custom-call(bf16[1024,512]{1,0:T(8,128)(2,1)S(1)} %copy-done.18, bf16[1024,512]{1,0:T(8,128)(2,1)S(1)} %copy-done.13, bf16[1024,1024]{1,0:T(8,128)(2,1)S(1)} %copy-done.9, f32[2,8,128]{2,1,0:T(8,128)S(1)} %bitcast.17, f32[2,136,128]{2,1,0:T(8,128)S(1)} %pad_maximum_fusion.table_ref), custom_call_target="tpu_custom_call" | custom-call | tf_op jit(solution)/shard_map/local/pallas_call | solution.py:347
  49.6 6.5 %shard_map.104 = bf16[2,256,2048]{2,1,0:T(8,128)(2,1)S(1)} custom-call(s32[2]{0:T(128)S(1)} %get-tuple-element.66.order_ref, s32[1]{0:T(128)} %bitcast.y_ref, f32[1024,1024]{1,0:T(8,128)} %get-tuple-element.29.local_ref, bf16[1024,512]{1,0:T(8,128)(2,1)S(1)} %get-tuple-element.30.qd_ref, bf16[256,512]{1,0:T(8,128)(2,1)S(1)} %get-tuple-element.33.keep_ref, ...), custom_call_target="tpu_custom_call" | custom-call | tf_op jit(solution)/shard_map/pallas_call | solution.py:383
  59.9 7.4 %collective-permute-start.11 = (bf16[256,1024]{1,0:T(8,128)(2,1)S(1)}, bf16[256,1024]{1,0:T(8,128)(2,1)S(1)}, u32[]{:S(2)}, u32[]{:S(2)}) collective-permute-start(bf16[256,1024]{1,0:T(8,128)(2,1)S(1)} %get-tuple-element.59), channel_id=1, source_target_pairs={{0,8},{4,12},{8,16},{12,20},{16,24},{20,28},{24,0},{28,4},{1,9},{5... | collective-permute-start | bytes 1572872 | tf_op jit(solution)/shard_map/ppermute | solution.py:281
  67.3 6.5 %shard_map.103 = bf16[2,256,2048]{2,1,0:T(8,128)(2,1)S(1)} custom-call(s32[2]{0:T(128)S(1)} %get-tuple-element.65.order_ref, s32[1]{0:T(128)} %bitcast.y_ref, f32[1024,1024]{1,0:T(8,128)} %get-tuple-element.29.local_ref, bf16[1024,512]{1,0:T(8,128)(2,1)S(1)} %get-tuple-element.30.qd_ref, bf16[256,512]{1,0:T(8,128)(2,1)S(1)} %get-tuple-element.33.keep_ref, ...), custom_call_target="tpu_custom_call" | custom-call | tf_op jit(solution)/shard_map/pallas_call | solution.py:383
  78.6 3.4 %collective-permute-start.12 = (bf16[256,1024]{1,0:T(8,128)(2,1)S(1)}, bf16[256,1024]{1,0:T(8,128)(2,1)S(1)}, u32[]{:S(2)}, u32[]{:S(2)}) collective-permute-start(bf16[256,1024]{1,0:T(8,128)(2,1)S(1)} %get-tuple-element.60.rest_4_.rest_2_), channel_id=1, source_target_pairs={{0,16},{4,20},{8,24},{12,28},{16,0},{20,4},{24,8},{28,12},{1,17},{... | collective-permute-start | bytes 1572872 | tf_op jit(solution)/shard_map/ppermute | solution.py:281
  83.5 21.8 %collective-permute-done.12.rest_6_.rest_4_ = bf16[256,1024]{1,0:T(8,128)(2,1)S(1)} collective-permute-done((bf16[256,1024]{1,0:T(8,128)(2,1)S(1)}, bf16[256,1024]{1,0:T(8,128)(2,1)S(1)}, u32[]{:S(2)}, u32[]{:S(2)}) %collective-permute-start.12) | collective-permute-done | bytes 524320 | tf_op jit(solution)/shard_map/ppermute | solution.py:281
  105.3 11.0 %collective-permute-start.19 = (bf16[1024,256]{1,0:T(8,128)(2,1)S(1)}, bf16[1024,256]{1,0:T(8,128)(2,1)S(1)}, u32[]{:S(2)}, u32[]{:S(2)}) collective-permute-start(bf16[1024,256]{1,0:T(8,128)(2,1)S(1)} %get-tuple-element.57), channel_id=1, source_target_pairs={{0,8},{4,12},{8,16},{12,20},{16,24},{20,28},{24,0},{28,4},{1,9},{5... | collective-permute-start | bytes 1572872 | tf_op jit(solution)/shard_map/ppermute | solution.py:281
  116.3 3.4 %collective-permute-start.20 = (bf16[1024,256]{1,0:T(8,128)(2,1)S(1)}, bf16[1024,256]{1,0:T(8,128)(2,1)S(1)}, u32[]{:S(2)}, u32[]{:S(2)}) collective-permute-start(bf16[1024,256]{1,0:T(8,128)(2,1)S(1)} %get-tuple-element.58.rest_2_.rest_1_), channel_id=1, source_target_pairs={{0,16},{4,20},{8,24},{12,28},{16,0},{20,4},{24,8},{28,12},{1,17},{... | collective-permute-start | bytes 1572872 | tf_op jit(solution)/shard_map/ppermute | solution.py:281
  125.0 7.0 %collective-permute-done.19.rest_3_.rest_2_ = bf16[1024,256]{1,0:T(8,128)(2,1)S(1)} collective-permute-done((bf16[1024,256]{1,0:T(8,128)(2,1)S(1)}, bf16[1024,256]{1,0:T(8,128)(2,1)S(1)}, u32[]{:S(2)}, u32[]{:S(2)}) %collective-permute-start.19) | collective-permute-done | bytes 524320 | tf_op jit(solution)/shard_map/ppermute | solution.py:281
  132.5 20.4 %collective-permute-done.20.rest_4_.rest_3_ = bf16[1024,256]{1,0:T(8,128)(2,1)S(1)} collective-permute-done((bf16[1024,256]{1,0:T(8,128)(2,1)S(1)}, bf16[1024,256]{1,0:T(8,128)(2,1)S(1)}, u32[]{:S(2)}, u32[]{:S(2)}) %collective-permute-start.20) | collective-permute-done | bytes 524320 | tf_op jit(solution)/shard_map/ppermute | solution.py:281
  155.6 11.2 %collective-permute-start.24 = (bf16[128,2048]{1,0:T(8,128)(2,1)S(1)}, bf16[128,2048]{1,0:T(8,128)(2,1)S(1)}, u32[]{:S(2)}, u32[]{:S(2)}) collective-permute-start(bf16[128,2048]{1,0:T(8,128)(2,1)S(1)} %get-tuple-element.62), channel_id=1, source_target_pairs={{0,8},{4,12},{8,0},{12,4},{16,24},{20,28},{24,16},{28,20},{1,9},{5... | collective-permute-start | bytes 1572872 | tf_op jit(solution)/shard_map/ppermute | solution.py:281
  168.3 10.7 %collective-permute-done.37.rest_3_.rest_2_ = bf16[1024,256]{1,0:T(8,128)(2,1)S(1)} collective-permute-done((bf16[1024,256]{1,0:T(8,128)(2,1)S(1)}, bf16[1024,256]{1,0:T(8,128)(2,1)S(1)}, u32[]{:S(2)}, u32[]{:S(2)}) %collective-permute-start.37) | collective-permute-done | bytes 524320 | tf_op jit(solution)/shard_map/ppermute | solution.py:281
  179.7 10.5 %collective-permute-done.38.rest_4_.rest_3_ = bf16[1024,256]{1,0:T(8,128)(2,1)S(1)} collective-permute-done((bf16[1024,256]{1,0:T(8,128)(2,1)S(1)}, bf16[1024,256]{1,0:T(8,128)(2,1)S(1)}, u32[]{:S(2)}, u32[]{:S(2)}) %collective-permute-start.38) | collective-permute-done | bytes 524320 | tf_op jit(solution)/shard_map/ppermute | solution.py:281
  191.5 8.9 %collective-permute-done.39.rest_5_.rest_4_ = bf16[1024,256]{1,0:T(8,128)(2,1)S(1)} collective-permute-done((bf16[1024,256]{1,0:T(8,128)(2,1)S(1)}, bf16[1024,256]{1,0:T(8,128)(2,1)S(1)}, u32[]{:S(2)}, u32[]{:S(2)}) %collective-permute-start.39) | collective-permute-done | bytes 524320 | tf_op jit(solution)/shard_map/ppermute | solution.py:281
  202.0 5.9 %collective-permute-start.30 = (bf16[128,2048]{1,0:T(8,128)(2,1)S(1)}, bf16[128,2048]{1,0:T(8,128)(2,1)}, u32[]{:S(2)}, u32[]{:S(2)}) collective-permute-start(bf16[128,2048]{1,0:T(8,128)(2,1)S(1)} %collective-permute-done.8.rest_1_), channel_id=1, source_target_pairs={{0,8},{4,12},{8,0},{12,4},{16,24},{20,28},{24,16},{28,20},{1,9},{5... | collective-permute-start | bytes 1572872 | tf_op jit(solution)/shard_map/ppermute | solution.py:281
  208.5 6.3 %collective-permute-done.29.rest_0_ = bf16[128,2048]{1,0:T(8,128)(2,1)S(1)} collective-permute-done((bf16[128,2048]{1,0:T(8,128)(2,1)S(1)}, bf16[128,2048]{1,0:T(8,128)(2,1)S(1)}, u32[]{:S(2)}, u32[]{:S(2)}) %collective-permute-start.29) | collective-permute-done | bytes 524320 | tf_op jit(solution)/shard_map/ppermute | solution.py:278
  214.7 5.6 %collective-permute-done.30.rest_1_ = bf16[128,2048]{1,0:T(8,128)(2,1)} collective-permute-done((bf16[128,2048]{1,0:T(8,128)(2,1)S(1)}, bf16[128,2048]{1,0:T(8,128)(2,1)}, u32[]{:S(2)}, u32[]{:S(2)}) %collective-permute-start.30) | collective-permute-done | bytes 524320 | tf_op jit(solution)/shard_map/ppermute | solution.py:281
  220.4 4.5 %up.6.rest_0_ = bf16[512,1024]{1,0:T(8,128)(2,1)} custom-call(s32[1]{0:T(128)} %bitcast.8.z_ref, bf16[128,2048]{1,0:T(8,128)(2,1)S(1)} %collective-permute-done.24.rest_0_, bf16[128,2048]{1,0:T(8,128)(2,1)S(1)} %collective-permute-done.25.rest_1_, bf16[128,2048]{1,0:T(8,128)(2,1)S(1)} %collective-permute-done.26.rest_2_, ...), custom_call_target="tpu_custom_call" | custom-call | tf_op jit(solution)/shard_map/up/pallas_call | solution.py:433
  230.7 4.5 %up.4.rest_0_ = bf16[512,1024]{1,0:T(8,128)(2,1)} custom-call(s32[1]{0:T(128)} %bitcast.8.z_ref, bf16[128,2048]{1,0:T(8,128)(2,1)S(1)} %collective-permute-done.7.rest_0_, bf16[128,2048]{1,0:T(8,128)(2,1)S(1)} %collective-permute-done.8.rest_1_, bf16[128,2048]{1,0:T(8,128)(2,1)S(1)} %collective-permute-done.9.rest_2_, ...), custom_call_target="tpu_custom_call" | custom-call | tf_op jit(solution)/shard_map/up/pallas_call | solution.py:433
  236.2 3.9 %up.5.rest_1_ = bf16[512,1024]{1,0:T(8,128)(2,1)S(1)} custom-call(s32[1]{0:T(128)} %bitcast.8.z_ref, bf16[256,2048]{1,0:T(8,128)(2,1)} %copy-done.14, bf16[256,2048]{1,0:T(8,128)(2,1)} %copy-done.21, bf16[256,1024]{1,0:T(8,128)(2,1)S(1)} %get-tuple-element.60.rest_4_.rest_2_, bf16[256,1024]{1,0:T(8,128)(2,1)S(1)} %collective-permute-done.11.rest_5_.rest_3_, ...), custom_call_target="tpu_custom_call" | custom-call | tf_op jit(solution)/shard_map/up/pallas_call | solution.py:433
  241.1 4.5 %down.6 = (bf16[512,1024]{1,0:T(8,128)(2,1)S(1)}, bf16[512,1024]{1,0:T(8,128)(2,1)}) custom-call(s32[1]{0:T(128)} %bitcast.8.z_ref, bf16[512,1024]{1,0:T(8,128)(2,1)S(1)} %copy-done, bf16[512,1024]{1,0:T(8,128)(2,1)} %copy-done.1, bf16[1024,256]{1,0:T(8,128)(2,1)S(1)} %get-tuple-element.58.rest_2_.rest_1_, ...), custom_call_target="tpu_custom_call" | custom-call | tf_op jit(solution)/shard_map/down/pallas_call | solution.py:446
  246.1 3.8 %down.9 = (bf16[512,1024]{1,0:T(8,128)(2,1)S(1)}, bf16[512,1024]{1,0:T(8,128)(2,1)S(1)}) custom-call(s32[1]{0:T(128)} %bitcast.8.z_ref, bf16[512,1024]{1,0:T(8,128)(2,1)S(1)} %copy-done, bf16[512,1024]{1,0:T(8,128)(2,1)} %copy-done.1, bf16[1024,256]{1,0:T(8,128)(2,1)S(1)} %collective-permute-done.36.rest_2_.rest_1_, ...), custom_call_target="tpu_custom_call" | custom-call | tf_op jit(solution)/shard_map/down/pallas_call | solution.py:446
  250.0 4.9 %up.7.rest_0_ = bf16[512,1024]{1,0:T(8,128)(2,1)} custom-call(s32[1]{0:T(128)} %bitcast.8.z_ref, bf16[128,2048]{1,0:T(8,128)(2,1)S(1)} %collective-permute-done.29.rest_0_, bf16[128,2048]{1,0:T(8,128)(2,1)} %collective-permute-done.30.rest_1_, bf16[128,2048]{1,0:T(8,128)(2,1)} %collective-permute-done.31.rest_2_, ...), custom_call_target="tpu_custom_call" | custom-call | tf_op jit(solution)/shard_map/up/pallas_call | solution.py:433
  269.0 9.8 %collective-permute-done.34 = bf16[256,1024]{1,0:T(8,128)(2,1)S(1)} collective-permute-done((bf16[256,1024]{1,0:T(8,128)(2,1)S(1)}, bf16[256,1024]{1,0:T(8,128)(2,1)S(1)}, u32[]{:S(2)}, u32[]{:S(2)}) %collective-permute-start.34) | collective-permute-done | bytes 524320 | tf_op jit(solution)/shard_map/ppermute | solution.py:278
  279.5 8.4 %collective-permute-done.44 = bf16[256,1024]{1,0:T(8,128)(2,1)S(1)} collective-permute-done((bf16[256,1024]{1,0:T(8,128)(2,1)S(1)}, bf16[256,1024]{1,0:T(8,128)(2,1)S(1)}, u32[]{:S(2)}, u32[]{:S(2)}) %collective-permute-start.44) | collective-permute-done | bytes 524320 | tf_op jit(solution)/shard_map/ppermute | solution.py:281
  289.6 9.1 %collective-permute-done.35 = bf16[256,1024]{1,0:T(8,128)(2,1)S(1)} collective-permute-done((bf16[256,1024]{1,0:T(8,128)(2,1)S(1)}, bf16[256,1024]{1,0:T(8,128)(2,1)S(1)}, u32[]{:S(2)}, u32[]{:S(2)}) %collective-permute-start.35) | collective-permute-done | bytes 524320 | tf_op jit(solution)/shard_map/ppermute | solution.py:281
  (151 shorter events, 66.3 us)
Async XLA Ops:
  59.9 23.1 %collective-permute-start.11 = (bf16[256,1024]{1,0:T(8,128)(2,1)S(1)}, bf16[256,1024]{1,0:T(8,128)(2,1)S(1)}, u32[]{:S(2)}, u32[]{:S(2)}) collective-permute-start(bf16[256,1024]{1,0:T(8,128)(2,1)S(1)} %get-tuple-element.59), channel_id=1, source_target_pairs={{0,8},{4,12},{8,16},{12,20},{16,24},{20,28},{24,0},{28,4},{1,9},{5... | collective-permute-start | bytes 1572872 | tf_op jit(solution)/shard_map/ppermute | solution.py:281
  74.1 45.6 %collective-permute-start.4 = (bf16[256,2048]{1,0:T(8,128)(2,1)S(1)}, bf16[256,2048]{1,0:T(8,128)(2,1)S(1)}, u32[]{:S(2)}, u32[]{:S(2)}) collective-permute-start(bf16[256,2048]{1,0:T(8,128)(2,1)S(1)} %get-tuple-element.55), channel_id=1, source_target_pairs={{0,1},{1,0},{2,3},{3,2},{4,5},{5,4},{6,7},{7,6},{8,9},{9,8},{10,11... | collective-permute-start | bytes 3145736 | tf_op jit(solution)/shard_map/ppermute | solution.py:278
  77.1 43.2 %collective-permute-start.6 = (bf16[256,2048]{1,0:T(8,128)(2,1)S(1)}, bf16[256,2048]{1,0:T(8,128)(2,1)S(1)}, u32[]{:S(2)}, u32[]{:S(2)}) collective-permute-start(bf16[256,2048]{1,0:T(8,128)(2,1)S(1)} %fusion), channel_id=1, source_target_pairs={{0,2},{1,3},{2,0},{3,1},{4,6},{5,7},{6,4},{7,5},{8,10},{9,11},{10,... | collective-permute-start | bytes 3145736 | tf_op jit(solution)/shard_map/ppermute | solution.py:278
  78.6 26.7 %collective-permute-start.12 = (bf16[256,1024]{1,0:T(8,128)(2,1)S(1)}, bf16[256,1024]{1,0:T(8,128)(2,1)S(1)}, u32[]{:S(2)}, u32[]{:S(2)}) collective-permute-start(bf16[256,1024]{1,0:T(8,128)(2,1)S(1)} %get-tuple-element.60.rest_4_.rest_2_), channel_id=1, source_target_pairs={{0,16},{4,20},{8,24},{12,28},{16,0},{20,4},{24,8},{28,12},{1,17},{... | collective-permute-start | bytes 1572872 | tf_op jit(solution)/shard_map/ppermute | solution.py:281
  82.0 34.3 %collective-permute-start.13 = (bf16[256,1024]{1,0:T(8,128)(2,1)S(1)}, bf16[256,1024]{1,0:T(8,128)(2,1)S(1)}, u32[]{:S(2)}, u32[]{:S(2)}) collective-permute-start(bf16[256,1024]{1,0:T(8,128)(2,1)S(1)} %get-tuple-element.59), channel_id=1, source_target_pairs={{0,24},{4,28},{8,0},{12,4},{16,8},{20,12},{24,16},{28,20},{1,25},{... | collective-permute-start | bytes 1572872 | tf_op jit(solution)/shard_map/ppermute | solution.py:281
  82.9 36.7 %collective-permute-start.14 = (bf16[256,1024]{1,0:T(8,128)(2,1)S(1)}, bf16[256,1024]{1,0:T(8,128)(2,1)S(1)}, u32[]{:S(2)}, u32[]{:S(2)}) collective-permute-start(bf16[256,1024]{1,0:T(8,128)(2,1)S(1)} %get-tuple-element.60.rest_4_.rest_2_), channel_id=1, source_target_pairs={{0,4},{4,0},{8,12},{12,8},{16,20},{20,16},{24,28},{28,24},{1,5},{5... | collective-permute-start | bytes 1572872 | tf_op jit(solution)/shard_map/ppermute | solution.py:281
  105.3 26.7 %collective-permute-start.19 = (bf16[1024,256]{1,0:T(8,128)(2,1)S(1)}, bf16[1024,256]{1,0:T(8,128)(2,1)S(1)}, u32[]{:S(2)}, u32[]{:S(2)}) collective-permute-start(bf16[1024,256]{1,0:T(8,128)(2,1)S(1)} %get-tuple-element.57), channel_id=1, source_target_pairs={{0,8},{4,12},{8,16},{12,20},{16,24},{20,28},{24,0},{28,4},{1,9},{5... | collective-permute-start | bytes 1572872 | tf_op jit(solution)/shard_map/ppermute | solution.py:281
  116.3 36.6 %collective-permute-start.20 = (bf16[1024,256]{1,0:T(8,128)(2,1)S(1)}, bf16[1024,256]{1,0:T(8,128)(2,1)S(1)}, u32[]{:S(2)}, u32[]{:S(2)}) collective-permute-start(bf16[1024,256]{1,0:T(8,128)(2,1)S(1)} %get-tuple-element.58.rest_2_.rest_1_), channel_id=1, source_target_pairs={{0,16},{4,20},{8,24},{12,28},{16,0},{20,4},{24,8},{28,12},{1,17},{... | collective-permute-start | bytes 1572872 | tf_op jit(solution)/shard_map/ppermute | solution.py:281
  119.7 33.8 %collective-permute-start.21 = (bf16[1024,256]{1,0:T(8,128)(2,1)S(1)}, bf16[1024,256]{1,0:T(8,128)(2,1)S(1)}, u32[]{:S(2)}, u32[]{:S(2)}) collective-permute-start(bf16[1024,256]{1,0:T(8,128)(2,1)S(1)} %get-tuple-element.57), channel_id=1, source_target_pairs={{0,24},{4,28},{8,0},{12,4},{16,8},{20,12},{24,16},{28,20},{1,25},{... | collective-permute-start | bytes 1572872 | tf_op jit(solution)/shard_map/ppermute | solution.py:281
  119.7 35.3 %collective-permute-start.36 = (bf16[1024,256]{1,0:T(8,128)(2,1)S(1)}, bf16[1024,256]{1,0:T(8,128)(2,1)S(1)}, u32[]{:S(2)}, u32[]{:S(2)}) collective-permute-start(bf16[1024,256]{1,0:T(8,128)(2,1)S(1)} %get-tuple-element.58.rest_2_.rest_1_), channel_id=1, source_target_pairs={{0,4},{4,0},{8,12},{12,8},{16,20},{20,16},{24,28},{28,24},{1,5},{5... | collective-permute-start | bytes 1572872 | tf_op jit(solution)/shard_map/ppermute | solution.py:281
  120.3 35.3 %collective-permute-start.15 = (bf16[256,1024]{1,0:T(8,128)(2,1)S(1)}, bf16[256,1024]{1,0:T(8,128)(2,1)S(1)}, u32[]{:S(2)}, u32[]{:S(2)}) collective-permute-start(bf16[256,1024]{1,0:T(8,128)(2,1)S(1)} %collective-permute-done.11.rest_5_.rest_3_), channel_id=1, source_target_pairs={{0,4},{4,0},{8,12},{12,8},{16,20},{20,16},{24,28},{28,24},{1,5},{5... | collective-permute-start | bytes 1572872 | tf_op jit(solution)/shard_map/ppermute | solution.py:281
  132.0 34.8 %collective-permute-start.16 = (bf16[256,1024]{1,0:T(8,128)(2,1)S(1)}, bf16[256,1024]{1,0:T(8,128)(2,1)S(1)}, u32[]{:S(2)}, u32[]{:S(2)}) collective-permute-start(bf16[256,1024]{1,0:T(8,128)(2,1)S(1)} %collective-permute-done.12.rest_6_.rest_4_), channel_id=1, source_target_pairs={{0,4},{4,0},{8,12},{12,8},{16,20},{20,16},{24,28},{28,24},{1,5},{5... | collective-permute-start | bytes 1572872 | tf_op jit(solution)/shard_map/ppermute | solution.py:281
  153.5 25.5 %collective-permute-start.37 = (bf16[1024,256]{1,0:T(8,128)(2,1)S(1)}, bf16[1024,256]{1,0:T(8,128)(2,1)S(1)}, u32[]{:S(2)}, u32[]{:S(2)}) collective-permute-start(bf16[1024,256]{1,0:T(8,128)(2,1)S(1)} %collective-permute-done.19.rest_3_.rest_2_), channel_id=1, source_target_pairs={{0,4},{4,0},{8,12},{12,8},{16,20},{20,16},{24,28},{28,24},{1,5},{5... | collective-permute-start | bytes 1572872 | tf_op jit(solution)/shard_map/ppermute | solution.py:281
  154.9 35.2 %collective-permute-start.38 = (bf16[1024,256]{1,0:T(8,128)(2,1)S(1)}, bf16[1024,256]{1,0:T(8,128)(2,1)S(1)}, u32[]{:S(2)}, u32[]{:S(2)}) collective-permute-start(bf16[1024,256]{1,0:T(8,128)(2,1)S(1)} %collective-permute-done.20.rest_4_.rest_3_), channel_id=1, source_target_pairs={{0,4},{4,0},{8,12},{12,8},{16,20},{20,16},{24,28},{28,24},{1,5},{5... | collective-permute-start | bytes 1572872 | tf_op jit(solution)/shard_map/ppermute | solution.py:281
  155.6 35.3 %collective-permute-start.24 = (bf16[128,2048]{1,0:T(8,128)(2,1)S(1)}, bf16[128,2048]{1,0:T(8,128)(2,1)S(1)}, u32[]{:S(2)}, u32[]{:S(2)}) collective-permute-start(bf16[128,2048]{1,0:T(8,128)(2,1)S(1)} %get-tuple-element.62), channel_id=1, source_target_pairs={{0,8},{4,12},{8,0},{12,4},{16,24},{20,28},{24,16},{28,20},{1,9},{5... | collective-permute-start | bytes 1572872 | tf_op jit(solution)/shard_map/ppermute | solution.py:281
  166.8 24.1 %collective-permute-start.25 = (bf16[128,2048]{1,0:T(8,128)(2,1)S(1)}, bf16[128,2048]{1,0:T(8,128)(2,1)S(1)}, u32[]{:S(2)}, u32[]{:S(2)}) collective-permute-start(bf16[128,2048]{1,0:T(8,128)(2,1)S(1)} %get-tuple-element.61), channel_id=1, source_target_pairs={{0,8},{4,12},{8,0},{12,4},{16,24},{20,28},{24,16},{28,20},{1,9},{5... | collective-permute-start | bytes 1572872 | tf_op jit(solution)/shard_map/ppermute | solution.py:281
  167.7 32.7 %collective-permute-start.39 = (bf16[1024,256]{1,0:T(8,128)(2,1)S(1)}, bf16[1024,256]{1,0:T(8,128)(2,1)S(1)}, u32[]{:S(2)}, u32[]{:S(2)}) collective-permute-start(bf16[1024,256]{1,0:T(8,128)(2,1)S(1)} %collective-permute-done.21.rest_5_.rest_4_), channel_id=1, source_target_pairs={{0,4},{4,0},{8,12},{12,8},{16,20},{20,16},{24,28},{28,24},{1,5},{5... | collective-permute-start | bytes 1572872 | tf_op jit(solution)/shard_map/ppermute | solution.py:281
  178.9 21.4 %collective-permute-start.8 = (bf16[128,2048]{1,0:T(8,128)(2,1)S(1)}, bf16[128,2048]{1,0:T(8,128)(2,1)S(1)}, u32[]{:S(2)}, u32[]{:S(2)}) collective-permute-start(bf16[128,2048]{1,0:T(8,128)(2,1)S(1)} %get-tuple-element.61), channel_id=1, source_target_pairs={{0,2},{1,3},{2,0},{3,1},{4,6},{5,7},{6,4},{7,5},{8,10},{9,11},{10,... | collective-permute-start | bytes 1572872 | tf_op jit(solution)/shard_map/ppermute | solution.py:278
  200.4 34.8 %collective-permute-start.18 = (bf16[256,2048]{1,0:T(8,128)(2,1)S(1)}, bf16[256,2048]{1,0:T(8,128)(2,1)S(1)}, u32[]{:S(2)}, u32[]{:S(2)}) collective-permute-start(bf16[256,2048]{1,0:T(8,128)(2,1)S(1)} %get-tuple-element.36.rest_0_), channel_id=1, source_target_pairs={{0,1},{1,0},{2,3},{3,2},{4,5},{5,4},{6,7},{7,6},{8,9},{9,8},{10,11... | collective-permute-start | bytes 3145736 | tf_op jit(solution)/shard_map/ppermute | solution.py:278
  202.0 18.3 %collective-permute-start.30 = (bf16[128,2048]{1,0:T(8,128)(2,1)S(1)}, bf16[128,2048]{1,0:T(8,128)(2,1)}, u32[]{:S(2)}, u32[]{:S(2)}) collective-permute-start(bf16[128,2048]{1,0:T(8,128)(2,1)S(1)} %collective-permute-done.8.rest_1_), channel_id=1, source_target_pairs={{0,8},{4,12},{8,0},{12,4},{16,24},{20,28},{24,16},{28,20},{1,9},{5... | collective-permute-start | bytes 1572872 | tf_op jit(solution)/shard_map/ppermute | solution.py:281
  207.9 20.2 %collective-permute-start.9 = (bf16[128,2048]{1,0:T(8,128)(2,1)S(1)}, bf16[128,2048]{1,0:T(8,128)(2,1)S(1)}, u32[]{:S(2)}, u32[]{:S(2)}) collective-permute-start(bf16[128,2048]{1,0:T(8,128)(2,1)S(1)} %collective-permute-done.7.rest_0_), channel_id=1, source_target_pairs={{0,1},{1,0},{2,3},{3,2},{4,5},{5,4},{6,7},{7,6},{8,9},{9,8},{10,11... | collective-permute-start | bytes 1572872 | tf_op jit(solution)/shard_map/ppermute | solution.py:278
  208.0 22.7 %collective-permute-start.10 = (bf16[128,2048]{1,0:T(8,128)(2,1)S(1)}, bf16[128,2048]{1,0:T(8,128)(2,1)S(1)}, u32[]{:S(2)}, u32[]{:S(2)}) collective-permute-start(bf16[128,2048]{1,0:T(8,128)(2,1)S(1)} %collective-permute-done.8.rest_1_), channel_id=1, source_target_pairs={{0,1},{1,0},{2,3},{3,2},{4,5},{5,4},{6,7},{7,6},{8,9},{9,8},{10,11... | collective-permute-start | bytes 1572872 | tf_op jit(solution)/shard_map/ppermute | solution.py:278
  214.7 35.2 %collective-permute-start.31 = (bf16[128,2048]{1,0:T(8,128)(2,1)S(1)}, bf16[128,2048]{1,0:T(8,128)(2,1)}, u32[]{:S(2)}, u32[]{:S(2)}) collective-permute-start(bf16[128,2048]{1,0:T(8,128)(2,1)S(1)} %collective-permute-done.29.rest_0_), channel_id=1, source_target_pairs={{0,1},{1,0},{2,3},{3,2},{4,5},{5,4},{6,7},{7,6},{8,9},{9,8},{10,11... | collective-permute-start | bytes 1572872 | tf_op jit(solution)/shard_map/ppermute | solution.py:278
  220.4 29.7 %collective-permute-start.32 = (bf16[128,2048]{1,0:T(8,128)(2,1)}, bf16[128,2048]{1,0:T(8,128)(2,1)}, u32[]{:S(2)}, u32[]{:S(2)}) collective-permute-start(bf16[128,2048]{1,0:T(8,128)(2,1)} %collective-permute-done.30.rest_1_), channel_id=1, source_target_pairs={{0,1},{1,0},{2,3},{3,2},{4,5},{5,4},{6,7},{7,6},{8,9},{9,8},{10,11... | collective-permute-start | bytes 1572872 | tf_op jit(solution)/shard_map/ppermute | solution.py:278
  228.1 29.8 %collective-permute-start.28 = (bf16[256,1024]{1,0:T(8,128)(2,1)}, bf16[256,1024]{1,0:T(8,128)(2,1)}, u32[]{:S(2)}, u32[]{:S(2)}) collective-permute-start(bf16[256,1024]{1,0:T(8,128)(2,1)} %get-tuple-element.42), channel_id=1, source_target_pairs={{0,1},{1,0},{2,3},{3,2},{4,5},{5,4},{6,7},{7,6},{8,9},{9,8},{10,11... | collective-permute-start | bytes 1572872 | tf_op jit(solution)/shard_map/ppermute | solution.py:278
  230.7 29.9 %collective-permute-start.41 = (bf16[256,1024]{1,0:T(8,128)(2,1)}, bf16[256,1024]{1,0:T(8,128)(2,1)}, u32[]{:S(2)}, u32[]{:S(2)}) collective-permute-start(bf16[256,1024]{1,0:T(8,128)(2,1)} %get-tuple-element.49), channel_id=1, source_target_pairs={{0,1},{1,0},{2,3},{3,2},{4,5},{5,4},{6,7},{7,6},{8,9},{9,8},{10,11... | collective-permute-start | bytes 1572872 | tf_op jit(solution)/shard_map/ppermute | solution.py:278
  245.6 20.2 %collective-permute-start.22 = (bf16[512,1024]{1,0:T(8,128)(2,1)}, bf16[512,1024]{1,0:T(8,128)(2,1)}, u32[]{:S(2)}, u32[]{:S(2)}) collective-permute-start(bf16[512,1024]{1,0:T(8,128)(2,1)} %get-tuple-element.38), channel_id=1, source_target_pairs={{0,1},{1,0},{2,3},{3,2},{4,5},{5,4},{6,7},{7,6},{8,9},{9,8},{10,11... | collective-permute-start | bytes 3145736 | tf_op jit(solution)/shard_map/ppermute | solution.py:278
  249.9 29.3 %collective-permute-start.40 = (bf16[512,1024]{1,0:T(8,128)(2,1)S(1)}, bf16[512,1024]{1,0:T(8,128)(2,1)S(1)}, u32[]{:S(2)}, u32[]{:S(2)}) collective-permute-start(bf16[512,1024]{1,0:T(8,128)(2,1)S(1)} %get-tuple-element.46), channel_id=1, source_target_pairs={{0,1},{1,0},{2,3},{3,2},{4,5},{5,4},{6,7},{7,6},{8,9},{9,8},{10,11... | collective-permute-start | bytes 3145736 | tf_op jit(solution)/shard_map/ppermute | solution.py:278
  261.8 37.1 %collective-permute-start.42 = (bf16[256,1024]{1,0:T(8,128)(2,1)S(1)}, bf16[256,1024]{1,0:T(8,128)(2,1)S(1)}, u32[]{:S(2)}, u32[]{:S(2)}) collective-permute-start(bf16[256,1024]{1,0:T(8,128)(2,1)S(1)} %convert_add_fusion.2), channel_id=1, source_target_pairs={{0,8},{4,12},{8,0},{12,4},{16,24},{20,28},{24,16},{28,20},{1,9},{5... | collective-permute-start | bytes 1572872 | tf_op jit(solution)/shard_map/ppermute | solution.py:281
  265.6 22.4 %collective-permute-start.44 = (bf16[256,1024]{1,0:T(8,128)(2,1)S(1)}, bf16[256,1024]{1,0:T(8,128)(2,1)S(1)}, u32[]{:S(2)}, u32[]{:S(2)}) collective-permute-start(bf16[256,1024]{1,0:T(8,128)(2,1)S(1)} %convert_add_fusion.1), channel_id=1, source_target_pairs={{0,8},{4,12},{8,0},{12,4},{16,24},{20,28},{24,16},{28,20},{1,9},{5... | collective-permute-start | bytes 1572872 | tf_op jit(solution)/shard_map/ppermute | solution.py:281
  268.3 21.3 %collective-permute-start.23 = (bf16[256,1024]{1,0:T(8,128)(2,1)S(1)}, bf16[256,1024]{1,0:T(8,128)(2,1)S(1)}, u32[]{:S(2)}, u32[]{:S(2)}) collective-permute-start(bf16[256,1024]{1,0:T(8,128)(2,1)S(1)} %convert_add_fusion.9), channel_id=1, source_target_pairs={{0,2},{1,3},{2,0},{3,1},{4,6},{5,7},{6,4},{7,5},{8,10},{9,11},{10,... | collective-permute-start | bytes 1572872 | tf_op jit(solution)/shard_map/ppermute | solution.py:278
  278.9 19.8 %collective-permute-start.35 = (bf16[256,1024]{1,0:T(8,128)(2,1)S(1)}, bf16[256,1024]{1,0:T(8,128)(2,1)S(1)}, u32[]{:S(2)}, u32[]{:S(2)}) collective-permute-start(bf16[256,1024]{1,0:T(8,128)(2,1)S(1)} %add_convert_fusion.2), channel_id=1, source_target_pairs={{0,8},{4,12},{8,0},{12,4},{16,24},{20,28},{24,16},{28,20},{1,9},{5... | collective-permute-start | bytes 1572872 | tf_op jit(solution)/shard_map/ppermute | solution.py:281
  (37 other events, 469.7 us)

commit v3 on v2

--- a/solution.py
+++ b/solution.py
@@ -440,7 +440,7 @@
                 name="up",
             )(*args)
 
-        def lowered(sources, side):
+        def lowered(sources, side, kinds):
             args = (z_word, *sources, *down[side * n_z : (side + 1) * n_z])
             tall = len(sources) * own_rows
             mine, others = pl.pallas_call(
@@ -454,7 +454,10 @@
             )(*args)
             others = swap_core(others)
             parts = [slice(i * own_rows, (i + 1) * own_rows) for i in range(len(sources))]
-            sums = [mine[part].astype(F32) + others[part].astype(F32) for part in parts]
+            sums = [
+                (mine[part].astype(F32) + others[part].astype(F32)).astype(kind)
+                for part, kind in zip(parts, kinds)
+            ]
             return lax.optimization_barrier(tuple(sums))
 
         near_x = range(1, n_x)
@@ -475,12 +478,12 @@
         def home(value, s):
             return shift_x(value.astype(BF), n_x - s).astype(F32)
 
-        (left_z,) = lowered([hidden["z"]], 0)
-        *left_x, left_sum = lowered(straight[:-2] + straight[-1:], 0)
-        left_c = lowered(corners, 0)
-        (right_z,) = lowered([hidden["z"]], 1)
-        *right_x, right_sum = lowered(straight[:-2] + straight[-1:], 1)
-        right_c = lowered(corners, 1)
+        (left_z,) = lowered([hidden["z"]], 0, [F32])
+        *left_x, left_sum = lowered(straight[:-2] + straight[-1:], 0, [BF] * (n_x - 1) + [F32])
+        left_c = lowered(corners, 0, [BF] * (n_x - 1))
+        (right_z,) = lowered([hidden["z"]], 1, [BF])
+        *right_x, right_sum = lowered(straight[:-2] + straight[-1:], 1, [F32] * n_x)
+        right_c = lowered(corners, 1, [BF] * (n_x - 1))
         for s in near_x:
             left_sum = left_sum + home(left_x[s - 1], s)
             left_z = left_z + home(left_c[s - 1], s)

time: 303 us -> 303 us (level)
  no operation moved by 1% of the time
where the time goes in v3:
time: 303 us
  waiting for transfers between devices  140 us (46%)
  starting transfers between devices  75.7 us (25%)
  Pallas kernels  61.2 us (20%)
  local copies, waits for them, and re-layouts  18.1 us (6%)
  other arithmetic  7.54 us (2%)
    ppermute x24, waiting for transfers between devices, over_sp(): return lax.ppermute(value, 'sp', pairs)  120 us
    ppermute x24, starting transfers between devices, over_sp(): return lax.ppermute(value, 'sp', pairs)  64.8 us
    ppermute x22, waiting for transfers between devices, over_tp(): return lax.ppermute(value, 'tp', [(t, turn(t)) for t in range(n_tp)])  19.6 us
    pallas_call x4, Pallas kernels, raised(): pl.pallas_call(functools.partial(up_kernel, planes=n_z, sources=len(sourc...  17.9 us
    unnamed x47, local copies, waits for them, and re-layouts  15.4 us
    pallas_call x6, Pallas kernels, lowered(): pl.pallas_call(functools.partial(down_kernel, planes=n_z), out_shape=(jax...  14.9 us
    pallas_call x2, Pallas kernels, projected(): pl.pallas_call(gate_kernel, out_shape=jax.ShapeDtypeStruct((count, own_ro...  13.1 us
    ppermute x22, starting transfers between devices, over_tp(): return lax.ppermute(value, 'tp', [(t, turn(t)) for t in range(n_tp)])  10.9 us
  transfers between devices with their start and end apart: 46, of which 18 were waited for; matrix products, arithmetic and copies ran while one was open for 3% of the time, Pallas kernels for 16%

profile of v3, /device:TPU:0, one launch (start us, length us, event | category | flops | bytes accessed | tf_op | source)
XLA Modules:
  0.0 302.5 jit_solution(2251220941940375547)
XLA Ops:
  3.9 3.2 %state.1 = (bf16[272,512]{1,0:T(8,128)(2,1)S(1)}, bf16[272,512]{1,0:T(8,128)(2,1)S(1)}) custom-call(s32[1]{0:T(128)} %bitcast.y_ref, bf16[1024,512]{1,0:T(8,128)(2,1)S(1)} %copy-done.12, bf16[1024,1024]{1,0:T(8,128)(2,1)S(1)} %copy-done.8, f32[2,8,128]{2,1,0:T(8,128)S(1)} %bitcast.16, f32[2,136,128]{2,1,0:T(8,128)S(1)} %pad_maximum_fusion.table_ref), custom_call_target="tpu_custom_call" | custom-call | tf_op jit(solution)/shard_map/state/pallas_call | solution.py:336
  10.2 6.6 %collective-permute-done.got_ref = bf16[272,512]{1,0:T(8,128)(2,1)S(1)} collective-permute-done((bf16[272,512]{1,0:T(8,128)(2,1)S(1)}, bf16[272,512]{1,0:T(8,128)(2,1)S(1)}, u32[]{:S(2)}, u32[]{:S(2)}) %collective-permute-start) | collective-permute-done | bytes 278560 | tf_op jit(solution)/shard_map/ppermute | solution.py:281
  17.0 3.7 %collective-permute-start.1 = (bf16[272,512]{1,0:T(8,128)(2,1)S(1)}, bf16[272,512]{1,0:T(8,128)(2,1)S(1)}, u32[]{:S(2)}, u32[]{:S(2)}) collective-permute-start(bf16[272,512]{1,0:T(8,128)(2,1)S(1)} %shard_map.100.plane_ref), channel_id=1, source_target_pairs={{0,8},{4,12},{8,16},{12,20},{16,24},{20,28},{1,9},{5,13},{9,17},{1... | collective-permute-start | bytes 835592 | tf_op jit(solution)/shard_map/ppermute | solution.py:281
  20.7 5.0 %collective-permute-done.1.rest_0_ = bf16[272,512]{1,0:T(8,128)(2,1)S(1)} collective-permute-done((bf16[272,512]{1,0:T(8,128)(2,1)S(1)}, bf16[272,512]{1,0:T(8,128)(2,1)S(1)}, u32[]{:S(2)}, u32[]{:S(2)}) %collective-permute-start.1) | collective-permute-done | bytes 278560 | tf_op jit(solution)/shard_map/ppermute | solution.py:281
  25.8 5.4 %collective-permute-start.2 = (bf16[272,512]{1,0:T(8,128)(2,1)S(1)}, bf16[272,512]{1,0:T(8,128)(2,1)S(1)}, u32[]{:S(2)}, u32[]{:S(2)}) collective-permute-start(bf16[272,512]{1,0:T(8,128)(2,1)S(1)} %shard_map.101), channel_id=1, source_target_pairs={{0,16},{4,20},{8,24},{12,28},{1,17},{5,21},{9,25},{13,29},{2,18},{... | collective-permute-start | bytes 835592 | tf_op jit(solution)/shard_map/ppermute | solution.py:281
  31.3 4.2 %collective-permute-done.2.rest_1_ = bf16[272,512]{1,0:T(8,128)(2,1)S(1)} collective-permute-done((bf16[272,512]{1,0:T(8,128)(2,1)S(1)}, bf16[272,512]{1,0:T(8,128)(2,1)S(1)}, u32[]{:S(2)}, u32[]{:S(2)}) %collective-permute-start.2) | collective-permute-done | bytes 278560 | tf_op jit(solution)/shard_map/ppermute | solution.py:281
  41.9 7.6 %local.1 = (f32[1024,1024]{1,0:T(8,128)}, bf16[1024,512]{1,0:T(8,128)(2,1)S(1)}) custom-call(bf16[1024,512]{1,0:T(8,128)(2,1)S(1)} %copy-done.18, bf16[1024,512]{1,0:T(8,128)(2,1)S(1)} %copy-done.13, bf16[1024,1024]{1,0:T(8,128)(2,1)S(1)} %copy-done.9, f32[2,8,128]{2,1,0:T(8,128)S(1)} %bitcast.17, f32[2,136,128]{2,1,0:T(8,128)S(1)} %pad_maximum_fusion.table_ref), custom_call_target="tpu_custom_call" | custom-call | tf_op jit(solution)/shard_map/local/pallas_call | solution.py:347
  49.6 6.5 %shard_map.104 = bf16[2,256,2048]{2,1,0:T(8,128)(2,1)S(1)} custom-call(s32[2]{0:T(128)S(1)} %get-tuple-element.68.order_ref, s32[1]{0:T(128)} %bitcast.y_ref, f32[1024,1024]{1,0:T(8,128)} %get-tuple-element.29.local_ref, bf16[1024,512]{1,0:T(8,128)(2,1)S(1)} %get-tuple-element.30.qd_ref, bf16[256,512]{1,0:T(8,128)(2,1)S(1)} %get-tuple-element.33.keep_ref, ...), custom_call_target="tpu_custom_call" | custom-call | tf_op jit(solution)/shard_map/pallas_call | solution.py:383
  59.8 7.4 %collective-permute-start.11 = (bf16[256,1024]{1,0:T(8,128)(2,1)S(1)}, bf16[256,1024]{1,0:T(8,128)(2,1)S(1)}, u32[]{:S(2)}, u32[]{:S(2)}) collective-permute-start(bf16[256,1024]{1,0:T(8,128)(2,1)S(1)} %get-tuple-element.61), channel_id=1, source_target_pairs={{0,8},{4,12},{8,16},{12,20},{16,24},{20,28},{24,0},{28,4},{1,9},{5... | collective-permute-start | bytes 1572872 | tf_op jit(solution)/shard_map/ppermute | solution.py:281
  67.3 6.5 %shard_map.103 = bf16[2,256,2048]{2,1,0:T(8,128)(2,1)S(1)} custom-call(s32[2]{0:T(128)S(1)} %get-tuple-element.67.order_ref, s32[1]{0:T(128)} %bitcast.y_ref, f32[1024,1024]{1,0:T(8,128)} %get-tuple-element.29.local_ref, bf16[1024,512]{1,0:T(8,128)(2,1)S(1)} %get-tuple-element.30.qd_ref, bf16[256,512]{1,0:T(8,128)(2,1)S(1)} %get-tuple-element.33.keep_ref, ...), custom_call_target="tpu_custom_call" | custom-call | tf_op jit(solution)/shard_map/pallas_call | solution.py:383
  78.6 3.4 %collective-permute-start.12 = (bf16[256,1024]{1,0:T(8,128)(2,1)S(1)}, bf16[256,1024]{1,0:T(8,128)(2,1)S(1)}, u32[]{:S(2)}, u32[]{:S(2)}) collective-permute-start(bf16[256,1024]{1,0:T(8,128)(2,1)S(1)} %get-tuple-element.62.rest_4_.rest_2_), channel_id=1, source_target_pairs={{0,16},{4,20},{8,24},{12,28},{16,0},{20,4},{24,8},{28,12},{1,17},{... | collective-permute-start | bytes 1572872 | tf_op jit(solution)/shard_map/ppermute | solution.py:281
  83.5 21.8 %collective-permute-done.12.rest_6_.rest_4_ = bf16[256,1024]{1,0:T(8,128)(2,1)S(1)} collective-permute-done((bf16[256,1024]{1,0:T(8,128)(2,1)S(1)}, bf16[256,1024]{1,0:T(8,128)(2,1)S(1)}, u32[]{:S(2)}, u32[]{:S(2)}) %collective-permute-start.12) | collective-permute-done | bytes 524320 | tf_op jit(solution)/shard_map/ppermute | solution.py:281
  105.3 11.0 %collective-permute-start.19 = (bf16[1024,256]{1,0:T(8,128)(2,1)S(1)}, bf16[1024,256]{1,0:T(8,128)(2,1)S(1)}, u32[]{:S(2)}, u32[]{:S(2)}) collective-permute-start(bf16[1024,256]{1,0:T(8,128)(2,1)S(1)} %get-tuple-element.59), channel_id=1, source_target_pairs={{0,8},{4,12},{8,16},{12,20},{16,24},{20,28},{24,0},{28,4},{1,9},{5... | collective-permute-start | bytes 1572872 | tf_op jit(solution)/shard_map/ppermute | solution.py:281
  116.2 3.4 %collective-permute-start.20 = (bf16[1024,256]{1,0:T(8,128)(2,1)S(1)}, bf16[1024,256]{1,0:T(8,128)(2,1)S(1)}, u32[]{:S(2)}, u32[]{:S(2)}) collective-permute-start(bf16[1024,256]{1,0:T(8,128)(2,1)S(1)} %get-tuple-element.60.rest_2_.rest_1_), channel_id=1, source_target_pairs={{0,16},{4,20},{8,24},{12,28},{16,0},{20,4},{24,8},{28,12},{1,17},{... | collective-permute-start | bytes 1572872 | tf_op jit(solution)/shard_map/ppermute | solution.py:281
  125.0 7.0 %collective-permute-done.19.rest_3_.rest_2_ = bf16[1024,256]{1,0:T(8,128)(2,1)S(1)} collective-permute-done((bf16[1024,256]{1,0:T(8,128)(2,1)S(1)}, bf16[1024,256]{1,0:T(8,128)(2,1)S(1)}, u32[]{:S(2)}, u32[]{:S(2)}) %collective-permute-start.19) | collective-permute-done | bytes 524320 | tf_op jit(solution)/shard_map/ppermute | solution.py:281
  132.5 20.4 %collective-permute-done.20.rest_4_.rest_3_ = bf16[1024,256]{1,0:T(8,128)(2,1)S(1)} collective-permute-done((bf16[1024,256]{1,0:T(8,128)(2,1)S(1)}, bf16[1024,256]{1,0:T(8,128)(2,1)S(1)}, u32[]{:S(2)}, u32[]{:S(2)}) %collective-permute-start.20) | collective-permute-done | bytes 524320 | tf_op jit(solution)/shard_map/ppermute | solution.py:281
  155.6 11.2 %collective-permute-start.24 = (bf16[128,2048]{1,0:T(8,128)(2,1)S(1)}, bf16[128,2048]{1,0:T(8,128)(2,1)S(1)}, u32[]{:S(2)}, u32[]{:S(2)}) collective-permute-start(bf16[128,2048]{1,0:T(8,128)(2,1)S(1)} %get-tuple-element.64), channel_id=1, source_target_pairs={{0,8},{4,12},{8,0},{12,4},{16,24},{20,28},{24,16},{28,20},{1,9},{5... | collective-permute-start | bytes 1572872 | tf_op jit(solution)/shard_map/ppermute | solution.py:281
  168.2 10.7 %collective-permute-done.37.rest_3_.rest_2_ = bf16[1024,256]{1,0:T(8,128)(2,1)S(1)} collective-permute-done((bf16[1024,256]{1,0:T(8,128)(2,1)S(1)}, bf16[1024,256]{1,0:T(8,128)(2,1)S(1)}, u32[]{:S(2)}, u32[]{:S(2)}) %collective-permute-start.37) | collective-permute-done | bytes 524320 | tf_op jit(solution)/shard_map/ppermute | solution.py:281
  179.7 10.5 %collective-permute-done.38.rest_4_.rest_3_ = bf16[1024,256]{1,0:T(8,128)(2,1)S(1)} collective-permute-done((bf16[1024,256]{1,0:T(8,128)(2,1)S(1)}, bf16[1024,256]{1,0:T(8,128)(2,1)S(1)}, u32[]{:S(2)}, u32[]{:S(2)}) %collective-permute-start.38) | collective-permute-done | bytes 524320 | tf_op jit(solution)/shard_map/ppermute | solution.py:281
  191.4 8.9 %collective-permute-done.39.rest_5_.rest_4_ = bf16[1024,256]{1,0:T(8,128)(2,1)S(1)} collective-permute-done((bf16[1024,256]{1,0:T(8,128)(2,1)S(1)}, bf16[1024,256]{1,0:T(8,128)(2,1)S(1)}, u32[]{:S(2)}, u32[]{:S(2)}) %collective-permute-start.39) | collective-permute-done | bytes 524320 | tf_op jit(solution)/shard_map/ppermute | solution.py:281
  202.0 5.9 %collective-permute-start.30 = (bf16[128,2048]{1,0:T(8,128)(2,1)S(1)}, bf16[128,2048]{1,0:T(8,128)(2,1)}, u32[]{:S(2)}, u32[]{:S(2)}) collective-permute-start(bf16[128,2048]{1,0:T(8,128)(2,1)S(1)} %collective-permute-done.8.rest_1_), channel_id=1, source_target_pairs={{0,8},{4,12},{8,0},{12,4},{16,24},{20,28},{24,16},{28,20},{1,9},{5... | collective-permute-start | bytes 1572872 | tf_op jit(solution)/shard_map/ppermute | solution.py:281
  208.4 6.3 %collective-permute-done.29.rest_0_ = bf16[128,2048]{1,0:T(8,128)(2,1)S(1)} collective-permute-done((bf16[128,2048]{1,0:T(8,128)(2,1)S(1)}, bf16[128,2048]{1,0:T(8,128)(2,1)S(1)}, u32[]{:S(2)}, u32[]{:S(2)}) %collective-permute-start.29) | collective-permute-done | bytes 524320 | tf_op jit(solution)/shard_map/ppermute | solution.py:278
  214.7 5.6 %collective-permute-done.30.rest_1_ = bf16[128,2048]{1,0:T(8,128)(2,1)} collective-permute-done((bf16[128,2048]{1,0:T(8,128)(2,1)S(1)}, bf16[128,2048]{1,0:T(8,128)(2,1)}, u32[]{:S(2)}, u32[]{:S(2)}) %collective-permute-start.30) | collective-permute-done | bytes 524320 | tf_op jit(solution)/shard_map/ppermute | solution.py:281
  220.3 4.5 %up.6.rest_0_ = bf16[512,1024]{1,0:T(8,128)(2,1)} custom-call(s32[1]{0:T(128)} %bitcast.8.z_ref, bf16[128,2048]{1,0:T(8,128)(2,1)S(1)} %collective-permute-done.24.rest_0_, bf16[128,2048]{1,0:T(8,128)(2,1)S(1)} %collective-permute-done.25.rest_1_, bf16[128,2048]{1,0:T(8,128)(2,1)S(1)} %collective-permute-done.26.rest_2_, ...), custom_call_target="tpu_custom_call" | custom-call | tf_op jit(solution)/shard_map/up/pallas_call | solution.py:433
  230.6 4.5 %up.4.rest_0_ = bf16[512,1024]{1,0:T(8,128)(2,1)} custom-call(s32[1]{0:T(128)} %bitcast.8.z_ref, bf16[128,2048]{1,0:T(8,128)(2,1)S(1)} %collective-permute-done.7.rest_0_, bf16[128,2048]{1,0:T(8,128)(2,1)S(1)} %collective-permute-done.8.rest_1_, bf16[128,2048]{1,0:T(8,128)(2,1)S(1)} %collective-permute-done.9.rest_2_, ...), custom_call_target="tpu_custom_call" | custom-call | tf_op jit(solution)/shard_map/up/pallas_call | solution.py:433
  236.2 3.9 %up.5.rest_1_ = bf16[512,1024]{1,0:T(8,128)(2,1)S(1)} custom-call(s32[1]{0:T(128)} %bitcast.8.z_ref, bf16[256,2048]{1,0:T(8,128)(2,1)} %copy-done.14, bf16[256,2048]{1,0:T(8,128)(2,1)} %copy-done.21, bf16[256,1024]{1,0:T(8,128)(2,1)S(1)} %get-tuple-element.62.rest_4_.rest_2_, bf16[256,1024]{1,0:T(8,128)(2,1)S(1)} %collective-permute-done.11.rest_5_.rest_3_, ...), custom_call_target="tpu_custom_call" | custom-call | tf_op jit(solution)/shard_map/up/pallas_call | solution.py:433
  241.1 4.5 %down.6 = (bf16[512,1024]{1,0:T(8,128)(2,1)S(1)}, bf16[512,1024]{1,0:T(8,128)(2,1)}) custom-call(s32[1]{0:T(128)} %bitcast.8.z_ref, bf16[512,1024]{1,0:T(8,128)(2,1)S(1)} %copy-done, bf16[512,1024]{1,0:T(8,128)(2,1)} %copy-done.1, bf16[1024,256]{1,0:T(8,128)(2,1)S(1)} %get-tuple-element.60.rest_2_.rest_1_, ...), custom_call_target="tpu_custom_call" | custom-call | tf_op jit(solution)/shard_map/down/pallas_call | solution.py:446
  246.0 3.8 %down.9 = (bf16[512,1024]{1,0:T(8,128)(2,1)S(1)}, bf16[512,1024]{1,0:T(8,128)(2,1)S(1)}) custom-call(s32[1]{0:T(128)} %bitcast.8.z_ref, bf16[512,1024]{1,0:T(8,128)(2,1)S(1)} %copy-done, bf16[512,1024]{1,0:T(8,128)(2,1)} %copy-done.1, bf16[1024,256]{1,0:T(8,128)(2,1)S(1)} %collective-permute-done.36.rest_2_.rest_1_, ...), custom_call_target="tpu_custom_call" | custom-call | tf_op jit(solution)/shard_map/down/pallas_call | solution.py:446
  250.0 4.9 %up.7.rest_0_ = bf16[512,1024]{1,0:T(8,128)(2,1)} custom-call(s32[1]{0:T(128)} %bitcast.8.z_ref, bf16[128,2048]{1,0:T(8,128)(2,1)S(1)} %collective-permute-done.29.rest_0_, bf16[128,2048]{1,0:T(8,128)(2,1)} %collective-permute-done.30.rest_1_, bf16[128,2048]{1,0:T(8,128)(2,1)} %collective-permute-done.31.rest_2_, ...), custom_call_target="tpu_custom_call" | custom-call | tf_op jit(solution)/shard_map/up/pallas_call | solution.py:433
  268.1 10.7 %collective-permute-done.34 = bf16[256,1024]{1,0:T(8,128)(2,1)S(1)} collective-permute-done((bf16[256,1024]{1,0:T(8,128)(2,1)S(1)}, bf16[256,1024]{1,0:T(8,128)(2,1)S(1)}, u32[]{:S(2)}, u32[]{:S(2)}) %collective-permute-start.34) | collective-permute-done | bytes 524320 | tf_op jit(solution)/shard_map/ppermute | solution.py:278
  279.5 8.4 %collective-permute-done.44 = bf16[256,1024]{1,0:T(8,128)(2,1)S(1)} collective-permute-done((bf16[256,1024]{1,0:T(8,128)(2,1)S(1)}, bf16[256,1024]{1,0:T(8,128)(2,1)S(1)}, u32[]{:S(2)}, u32[]{:S(2)}) %collective-permute-start.44) | collective-permute-done | bytes 524320 | tf_op jit(solution)/shard_map/ppermute | solution.py:281
  289.5 9.1 %collective-permute-done.35 = bf16[256,1024]{1,0:T(8,128)(2,1)S(1)} collective-permute-done((bf16[256,1024]{1,0:T(8,128)(2,1)S(1)}, bf16[256,1024]{1,0:T(8,128)(2,1)S(1)}, u32[]{:S(2)}, u32[]{:S(2)}) %collective-permute-start.35) | collective-permute-done | bytes 524320 | tf_op jit(solution)/shard_map/ppermute | solution.py:281
  (150 shorter events, 65.4 us)
Async XLA Ops:
  59.8 23.0 %collective-permute-start.11 = (bf16[256,1024]{1,0:T(8,128)(2,1)S(1)}, bf16[256,1024]{1,0:T(8,128)(2,1)S(1)}, u32[]{:S(2)}, u32[]{:S(2)}) collective-permute-start(bf16[256,1024]{1,0:T(8,128)(2,1)S(1)} %get-tuple-element.61), channel_id=1, source_target_pairs={{0,8},{4,12},{8,16},{12,20},{16,24},{20,28},{24,0},{28,4},{1,9},{5... | collective-permute-start | bytes 1572872 | tf_op jit(solution)/shard_map/ppermute | solution.py:281
  74.1 45.6 %collective-permute-start.4 = (bf16[256,2048]{1,0:T(8,128)(2,1)S(1)}, bf16[256,2048]{1,0:T(8,128)(2,1)S(1)}, u32[]{:S(2)}, u32[]{:S(2)}) collective-permute-start(bf16[256,2048]{1,0:T(8,128)(2,1)S(1)} %get-tuple-element.57), channel_id=1, source_target_pairs={{0,1},{1,0},{2,3},{3,2},{4,5},{5,4},{6,7},{7,6},{8,9},{9,8},{10,11... | collective-permute-start | bytes 3145736 | tf_op jit(solution)/shard_map/ppermute | solution.py:278
  77.0 43.2 %collective-permute-start.6 = (bf16[256,2048]{1,0:T(8,128)(2,1)S(1)}, bf16[256,2048]{1,0:T(8,128)(2,1)S(1)}, u32[]{:S(2)}, u32[]{:S(2)}) collective-permute-start(bf16[256,2048]{1,0:T(8,128)(2,1)S(1)} %fusion), channel_id=1, source_target_pairs={{0,2},{1,3},{2,0},{3,1},{4,6},{5,7},{6,4},{7,5},{8,10},{9,11},{10,... | collective-permute-start | bytes 3145736 | tf_op jit(solution)/shard_map/ppermute | solution.py:278
  78.6 26.7 %collective-permute-start.12 = (bf16[256,1024]{1,0:T(8,128)(2,1)S(1)}, bf16[256,1024]{1,0:T(8,128)(2,1)S(1)}, u32[]{:S(2)}, u32[]{:S(2)}) collective-permute-start(bf16[256,1024]{1,0:T(8,128)(2,1)S(1)} %get-tuple-element.62.rest_4_.rest_2_), channel_id=1, source_target_pairs={{0,16},{4,20},{8,24},{12,28},{16,0},{20,4},{24,8},{28,12},{1,17},{... | collective-permute-start | bytes 1572872 | tf_op jit(solution)/shard_map/ppermute | solution.py:281
  81.9 34.3 %collective-permute-start.13 = (bf16[256,1024]{1,0:T(8,128)(2,1)S(1)}, bf16[256,1024]{1,0:T(8,128)(2,1)S(1)}, u32[]{:S(2)}, u32[]{:S(2)}) collective-permute-start(bf16[256,1024]{1,0:T(8,128)(2,1)S(1)} %get-tuple-element.61), channel_id=1, source_target_pairs={{0,24},{4,28},{8,0},{12,4},{16,8},{20,12},{24,16},{28,20},{1,25},{... | collective-permute-start | bytes 1572872 | tf_op jit(solution)/shard_map/ppermute | solution.py:281
  82.9 36.7 %collective-permute-start.14 = (bf16[256,1024]{1,0:T(8,128)(2,1)S(1)}, bf16[256,1024]{1,0:T(8,128)(2,1)S(1)}, u32[]{:S(2)}, u32[]{:S(2)}) collective-permute-start(bf16[256,1024]{1,0:T(8,128)(2,1)S(1)} %get-tuple-element.62.rest_4_.rest_2_), channel_id=1, source_target_pairs={{0,4},{4,0},{8,12},{12,8},{16,20},{20,16},{24,28},{28,24},{1,5},{5... | collective-permute-start | bytes 1572872 | tf_op jit(solution)/shard_map/ppermute | solution.py:281
  105.3 26.7 %collective-permute-start.19 = (bf16[1024,256]{1,0:T(8,128)(2,1)S(1)}, bf16[1024,256]{1,0:T(8,128)(2,1)S(1)}, u32[]{:S(2)}, u32[]{:S(2)}) collective-permute-start(bf16[1024,256]{1,0:T(8,128)(2,1)S(1)} %get-tuple-element.59), channel_id=1, source_target_pairs={{0,8},{4,12},{8,16},{12,20},{16,24},{20,28},{24,0},{28,4},{1,9},{5... | collective-permute-start | bytes 1572872 | tf_op jit(solution)/shard_map/ppermute | solution.py:281
  116.2 36.6 %collective-permute-start.20 = (bf16[1024,256]{1,0:T(8,128)(2,1)S(1)}, bf16[1024,256]{1,0:T(8,128)(2,1)S(1)}, u32[]{:S(2)}, u32[]{:S(2)}) collective-permute-start(bf16[1024,256]{1,0:T(8,128)(2,1)S(1)} %get-tuple-element.60.rest_2_.rest_1_), channel_id=1, source_target_pairs={{0,16},{4,20},{8,24},{12,28},{16,0},{20,4},{24,8},{28,12},{1,17},{... | collective-permute-start | bytes 1572872 | tf_op jit(solution)/shard_map/ppermute | solution.py:281
  119.6 33.8 %collective-permute-start.21 = (bf16[1024,256]{1,0:T(8,128)(2,1)S(1)}, bf16[1024,256]{1,0:T(8,128)(2,1)S(1)}, u32[]{:S(2)}, u32[]{:S(2)}) collective-permute-start(bf16[1024,256]{1,0:T(8,128)(2,1)S(1)} %get-tuple-element.59), channel_id=1, source_target_pairs={{0,24},{4,28},{8,0},{12,4},{16,8},{20,12},{24,16},{28,20},{1,25},{... | collective-permute-start | bytes 1572872 | tf_op jit(solution)/shard_map/ppermute | solution.py:281
  119.6 35.3 %collective-permute-start.36 = (bf16[1024,256]{1,0:T(8,128)(2,1)S(1)}, bf16[1024,256]{1,0:T(8,128)(2,1)S(1)}, u32[]{:S(2)}, u32[]{:S(2)}) collective-permute-start(bf16[1024,256]{1,0:T(8,128)(2,1)S(1)} %get-tuple-element.60.rest_2_.rest_1_), channel_id=1, source_target_pairs={{0,4},{4,0},{8,12},{12,8},{16,20},{20,16},{24,28},{28,24},{1,5},{5... | collective-permute-start | bytes 1572872 | tf_op jit(solution)/shard_map/ppermute | solution.py:281
  120.2 35.3 %collective-permute-start.15 = (bf16[256,1024]{1,0:T(8,128)(2,1)S(1)}, bf16[256,1024]{1,0:T(8,128)(2,1)S(1)}, u32[]{:S(2)}, u32[]{:S(2)}) collective-permute-start(bf16[256,1024]{1,0:T(8,128)(2,1)S(1)} %collective-permute-done.11.rest_5_.rest_3_), channel_id=1, source_target_pairs={{0,4},{4,0},{8,12},{12,8},{16,20},{20,16},{24,28},{28,24},{1,5},{5... | collective-permute-start | bytes 1572872 | tf_op jit(solution)/shard_map/ppermute | solution.py:281
  132.0 34.8 %collective-permute-start.16 = (bf16[256,1024]{1,0:T(8,128)(2,1)S(1)}, bf16[256,1024]{1,0:T(8,128)(2,1)S(1)}, u32[]{:S(2)}, u32[]{:S(2)}) collective-permute-start(bf16[256,1024]{1,0:T(8,128)(2,1)S(1)} %collective-permute-done.12.rest_6_.rest_4_), channel_id=1, source_target_pairs={{0,4},{4,0},{8,12},{12,8},{16,20},{20,16},{24,28},{28,24},{1,5},{5... | collective-permute-start | bytes 1572872 | tf_op jit(solution)/shard_map/ppermute | solution.py:281
  153.4 25.5 %collective-permute-start.37 = (bf16[1024,256]{1,0:T(8,128)(2,1)S(1)}, bf16[1024,256]{1,0:T(8,128)(2,1)S(1)}, u32[]{:S(2)}, u32[]{:S(2)}) collective-permute-start(bf16[1024,256]{1,0:T(8,128)(2,1)S(1)} %collective-permute-done.19.rest_3_.rest_2_), channel_id=1, source_target_pairs={{0,4},{4,0},{8,12},{12,8},{16,20},{20,16},{24,28},{28,24},{1,5},{5... | collective-permute-start | bytes 1572872 | tf_op jit(solution)/shard_map/ppermute | solution.py:281
  154.9 35.2 %collective-permute-start.38 = (bf16[1024,256]{1,0:T(8,128)(2,1)S(1)}, bf16[1024,256]{1,0:T(8,128)(2,1)S(1)}, u32[]{:S(2)}, u32[]{:S(2)}) collective-permute-start(bf16[1024,256]{1,0:T(8,128)(2,1)S(1)} %collective-permute-done.20.rest_4_.rest_3_), channel_id=1, source_target_pairs={{0,4},{4,0},{8,12},{12,8},{16,20},{20,16},{24,28},{28,24},{1,5},{5... | collective-permute-start | bytes 1572872 | tf_op jit(solution)/shard_map/ppermute | solution.py:281
  155.6 35.4 %collective-permute-start.24 = (bf16[128,2048]{1,0:T(8,128)(2,1)S(1)}, bf16[128,2048]{1,0:T(8,128)(2,1)S(1)}, u32[]{:S(2)}, u32[]{:S(2)}) collective-permute-start(bf16[128,2048]{1,0:T(8,128)(2,1)S(1)} %get-tuple-element.64), channel_id=1, source_target_pairs={{0,8},{4,12},{8,0},{12,4},{16,24},{20,28},{24,16},{28,20},{1,9},{5... | collective-permute-start | bytes 1572872 | tf_op jit(solution)/shard_map/ppermute | solution.py:281
  166.8 24.1 %collective-permute-start.25 = (bf16[128,2048]{1,0:T(8,128)(2,1)S(1)}, bf16[128,2048]{1,0:T(8,128)(2,1)S(1)}, u32[]{:S(2)}, u32[]{:S(2)}) collective-permute-start(bf16[128,2048]{1,0:T(8,128)(2,1)S(1)} %get-tuple-element.63), channel_id=1, source_target_pairs={{0,8},{4,12},{8,0},{12,4},{16,24},{20,28},{24,16},{28,20},{1,9},{5... | collective-permute-start | bytes 1572872 | tf_op jit(solution)/shard_map/ppermute | solution.py:281
  167.7 32.7 %collective-permute-start.39 = (bf16[1024,256]{1,0:T(8,128)(2,1)S(1)}, bf16[1024,256]{1,0:T(8,128)(2,1)S(1)}, u32[]{:S(2)}, u32[]{:S(2)}) collective-permute-start(bf16[1024,256]{1,0:T(8,128)(2,1)S(1)} %collective-permute-done.21.rest_5_.rest_4_), channel_id=1, source_target_pairs={{0,4},{4,0},{8,12},{12,8},{16,20},{20,16},{24,28},{28,24},{1,5},{5... | collective-permute-start | bytes 1572872 | tf_op jit(solution)/shard_map/ppermute | solution.py:281
  178.9 21.4 %collective-permute-start.8 = (bf16[128,2048]{1,0:T(8,128)(2,1)S(1)}, bf16[128,2048]{1,0:T(8,128)(2,1)S(1)}, u32[]{:S(2)}, u32[]{:S(2)}) collective-permute-start(bf16[128,2048]{1,0:T(8,128)(2,1)S(1)} %get-tuple-element.63), channel_id=1, source_target_pairs={{0,2},{1,3},{2,0},{3,1},{4,6},{5,7},{6,4},{7,5},{8,10},{9,11},{10,... | collective-permute-start | bytes 1572872 | tf_op jit(solution)/shard_map/ppermute | solution.py:278
  200.3 34.8 %collective-permute-start.18 = (bf16[256,2048]{1,0:T(8,128)(2,1)S(1)}, bf16[256,2048]{1,0:T(8,128)(2,1)S(1)}, u32[]{:S(2)}, u32[]{:S(2)}) collective-permute-start(bf16[256,2048]{1,0:T(8,128)(2,1)S(1)} %get-tuple-element.36.rest_0_), channel_id=1, source_target_pairs={{0,1},{1,0},{2,3},{3,2},{4,5},{5,4},{6,7},{7,6},{8,9},{9,8},{10,11... | collective-permute-start | bytes 3145736 | tf_op jit(solution)/shard_map/ppermute | solution.py:278
  202.0 18.3 %collective-permute-start.30 = (bf16[128,2048]{1,0:T(8,128)(2,1)S(1)}, bf16[128,2048]{1,0:T(8,128)(2,1)}, u32[]{:S(2)}, u32[]{:S(2)}) collective-permute-start(bf16[128,2048]{1,0:T(8,128)(2,1)S(1)} %collective-permute-done.8.rest_1_), channel_id=1, source_target_pairs={{0,8},{4,12},{8,0},{12,4},{16,24},{20,28},{24,16},{28,20},{1,9},{5... | collective-permute-start | bytes 1572872 | tf_op jit(solution)/shard_map/ppermute | solution.py:281
  207.9 20.2 %collective-permute-start.9 = (bf16[128,2048]{1,0:T(8,128)(2,1)S(1)}, bf16[128,2048]{1,0:T(8,128)(2,1)S(1)}, u32[]{:S(2)}, u32[]{:S(2)}) collective-permute-start(bf16[128,2048]{1,0:T(8,128)(2,1)S(1)} %collective-permute-done.7.rest_0_), channel_id=1, source_target_pairs={{0,1},{1,0},{2,3},{3,2},{4,5},{5,4},{6,7},{7,6},{8,9},{9,8},{10,11... | collective-permute-start | bytes 1572872 | tf_op jit(solution)/shard_map/ppermute | solution.py:278
  207.9 22.7 %collective-permute-start.10 = (bf16[128,2048]{1,0:T(8,128)(2,1)S(1)}, bf16[128,2048]{1,0:T(8,128)(2,1)S(1)}, u32[]{:S(2)}, u32[]{:S(2)}) collective-permute-start(bf16[128,2048]{1,0:T(8,128)(2,1)S(1)} %collective-permute-done.8.rest_1_), channel_id=1, source_target_pairs={{0,1},{1,0},{2,3},{3,2},{4,5},{5,4},{6,7},{7,6},{8,9},{9,8},{10,11... | collective-permute-start | bytes 1572872 | tf_op jit(solution)/shard_map/ppermute | solution.py:278
  214.7 35.1 %collective-permute-start.31 = (bf16[128,2048]{1,0:T(8,128)(2,1)S(1)}, bf16[128,2048]{1,0:T(8,128)(2,1)}, u32[]{:S(2)}, u32[]{:S(2)}) collective-permute-start(bf16[128,2048]{1,0:T(8,128)(2,1)S(1)} %collective-permute-done.29.rest_0_), channel_id=1, source_target_pairs={{0,1},{1,0},{2,3},{3,2},{4,5},{5,4},{6,7},{7,6},{8,9},{9,8},{10,11... | collective-permute-start | bytes 1572872 | tf_op jit(solution)/shard_map/ppermute | solution.py:278
  220.3 29.7 %collective-permute-start.32 = (bf16[128,2048]{1,0:T(8,128)(2,1)}, bf16[128,2048]{1,0:T(8,128)(2,1)}, u32[]{:S(2)}, u32[]{:S(2)}) collective-permute-start(bf16[128,2048]{1,0:T(8,128)(2,1)} %collective-permute-done.30.rest_1_), channel_id=1, source_target_pairs={{0,1},{1,0},{2,3},{3,2},{4,5},{5,4},{6,7},{7,6},{8,9},{9,8},{10,11... | collective-permute-start | bytes 1572872 | tf_op jit(solution)/shard_map/ppermute | solution.py:278
  228.1 29.8 %collective-permute-start.28 = (bf16[256,1024]{1,0:T(8,128)(2,1)}, bf16[256,1024]{1,0:T(8,128)(2,1)}, u32[]{:S(2)}, u32[]{:S(2)}) collective-permute-start(bf16[256,1024]{1,0:T(8,128)(2,1)} %get-tuple-element.42), channel_id=1, source_target_pairs={{0,1},{1,0},{2,3},{3,2},{4,5},{5,4},{6,7},{7,6},{8,9},{9,8},{10,11... | collective-permute-start | bytes 1572872 | tf_op jit(solution)/shard_map/ppermute | solution.py:278
  230.6 29.9 %collective-permute-start.41 = (bf16[256,1024]{1,0:T(8,128)(2,1)}, bf16[256,1024]{1,0:T(8,128)(2,1)}, u32[]{:S(2)}, u32[]{:S(2)}) collective-permute-start(bf16[256,1024]{1,0:T(8,128)(2,1)} %get-tuple-element.49), channel_id=1, source_target_pairs={{0,1},{1,0},{2,3},{3,2},{4,5},{5,4},{6,7},{7,6},{8,9},{9,8},{10,11... | collective-permute-start | bytes 1572872 | tf_op jit(solution)/shard_map/ppermute | solution.py:278
  245.6 20.2 %collective-permute-start.22 = (bf16[512,1024]{1,0:T(8,128)(2,1)}, bf16[512,1024]{1,0:T(8,128)(2,1)}, u32[]{:S(2)}, u32[]{:S(2)}) collective-permute-start(bf16[512,1024]{1,0:T(8,128)(2,1)} %get-tuple-element.38), channel_id=1, source_target_pairs={{0,1},{1,0},{2,3},{3,2},{4,5},{5,4},{6,7},{7,6},{8,9},{9,8},{10,11... | collective-permute-start | bytes 3145736 | tf_op jit(solution)/shard_map/ppermute | solution.py:278
  249.8 29.3 %collective-permute-start.40 = (bf16[512,1024]{1,0:T(8,128)(2,1)S(1)}, bf16[512,1024]{1,0:T(8,128)(2,1)S(1)}, u32[]{:S(2)}, u32[]{:S(2)}) collective-permute-start(bf16[512,1024]{1,0:T(8,128)(2,1)S(1)} %get-tuple-element.46), channel_id=1, source_target_pairs={{0,1},{1,0},{2,3},{3,2},{4,5},{5,4},{6,7},{7,6},{8,9},{9,8},{10,11... | collective-permute-start | bytes 3145736 | tf_op jit(solution)/shard_map/ppermute | solution.py:278
  261.8 37.1 %collective-permute-start.42 = (bf16[256,1024]{1,0:T(8,128)(2,1)S(1)}, bf16[256,1024]{1,0:T(8,128)(2,1)S(1)}, u32[]{:S(2)}, u32[]{:S(2)}) collective-permute-start(bf16[256,1024]{1,0:T(8,128)(2,1)S(1)} %add_convert_fusion.3), channel_id=1, source_target_pairs={{0,8},{4,12},{8,0},{12,4},{16,24},{20,28},{24,16},{28,20},{1,9},{5... | collective-permute-start | bytes 1572872 | tf_op jit(solution)/shard_map/ppermute | solution.py:281
  265.5 22.4 %collective-permute-start.44 = (bf16[256,1024]{1,0:T(8,128)(2,1)S(1)}, bf16[256,1024]{1,0:T(8,128)(2,1)S(1)}, u32[]{:S(2)}, u32[]{:S(2)}) collective-permute-start(bf16[256,1024]{1,0:T(8,128)(2,1)S(1)} %add_convert_fusion.2), channel_id=1, source_target_pairs={{0,8},{4,12},{8,0},{12,4},{16,24},{20,28},{24,16},{28,20},{1,9},{5... | collective-permute-start | bytes 1572872 | tf_op jit(solution)/shard_map/ppermute | solution.py:281
  267.4 22.1 %collective-permute-start.23 = (bf16[256,1024]{1,0:T(8,128)(2,1)S(1)}, bf16[256,1024]{1,0:T(8,128)(2,1)S(1)}, u32[]{:S(2)}, u32[]{:S(2)}) collective-permute-start(bf16[256,1024]{1,0:T(8,128)(2,1)S(1)} %get-tuple-element.40), channel_id=1, source_target_pairs={{0,2},{1,3},{2,0},{3,1},{4,6},{5,7},{6,4},{7,5},{8,10},{9,11},{10,... | collective-permute-start | bytes 1572872 | tf_op jit(solution)/shard_map/ppermute | solution.py:278
  278.9 19.7 %collective-permute-start.35 = (bf16[256,1024]{1,0:T(8,128)(2,1)S(1)}, bf16[256,1024]{1,0:T(8,128)(2,1)S(1)}, u32[]{:S(2)}, u32[]{:S(2)}) collective-permute-start(bf16[256,1024]{1,0:T(8,128)(2,1)S(1)} %add_convert_fusion.4), channel_id=1, source_target_pairs={{0,8},{4,12},{8,0},{12,4},{16,24},{20,28},{24,16},{28,20},{1,9},{5... | collective-permute-start | bytes 1572872 | tf_op jit(solution)/shard_map/ppermute | solution.py:281
  (37 other events, 469.6 us)
